TPU v7x, 32 devices: a whole 2x2x4 slice. The times are simulated.
32 devices in a mesh: grp: 2 (over x), tp: 16 (over z, y, core).
Axes of the slice: x: 2, y: 2, z: 4, core: 2. Of those that a mesh axis runs over, the one named last changes fastest.
Arguments:
- stream_in: bfloat16 [64, 4, 4096], P('grp'), parts along dimension 0, may hold values from -6 to 6
- state_in: float32 [2, 64, 8, 256, 256], P(None, 'grp', None, 'tp'), parts along dimension 1, may hold values from -0.8 to 0.8
- norm_gain: bfloat16 [2, 4096], replicated, may hold values from 0.099609375 to 1.8984375
- query_weight: bfloat16 [2, 4096, 2048], P(None, None, 'tp'), may hold values from -0.09375 to 0.09375
- key_weight: bfloat16 [2, 4096, 2048], P(None, None, 'tp'), may hold values from -0.09375 to 0.09375
- value_weight: bfloat16 [2, 4096, 8, 256], P(None, None, None, 'tp'), as said below
- gate_weight: bfloat16 [2, 4096, 8, 256], P(None, None, None, 'tp'), may hold values from -0.09375 to 0.09375
- group_gain: bfloat16 [2, 8, 256], P(None, None, 'tp'), may hold values from 0.099609375 to 1.8984375
- output_weight: bfloat16 [2, 8, 256, 4096], P(None, None, 'tp'), may hold values from -0.375 to 0.375
Outputs:
- stream_out: bfloat16 [64, 4, 4096], P('grp', None, 'tp'), parts along dimension 0
- state_out: float32 [2, 64, 8, 256, 256], P(None, 'grp', None, 'tp'), parts along dimension 1
There are 2 independent parts, one for each index of `grp`. A program takes and returns all parts, laid end to end along the dimension named above; an argument that names none is the same for every part. Nothing has to cross between parts.
Inputs may be any that keep to these rules, and one draw needn't show every extreme that they name: `value_weight`: real values; column scales of the value projection differ.
All inputs are finite; a program needn't handle non-finite values.
Results may differ from a plain program's by a relative error of at most 0.024.
Values may be sent and summed in bfloat16 or wider, within the bound.
A program may use at most 64 MiB of HBM per device.

v0:
```python
import functools

import jax
import jax.numpy as jnp
import numpy as np
from jax import lax
from jax.experimental import pallas as pl
from jax.experimental.pallas import tpu as pltpu
from jax.sharding import PartitionSpec as P

HEAD_DIM = 256
PAST = 1024


EPS_RMS = 1e-06
EPS_GROUP = 1e-05
ROTARY_BASE = 10000.0


def log_decays(count):
    return jnp.log(1.0 - jnp.power(2.0, -5.0 - jnp.arange(count, dtype=jnp.float32)))


def decay_tables(log_gamma, count):
    steps = jnp.arange(count, dtype=jnp.float32)
    gap = steps[:, None] - steps[None, :]
    intra = jnp.where(
        gap[None] >= 0, jnp.exp(log_gamma[:, None, None] * jnp.maximum(gap, 0.0)[None]), 0.0
    )
    q_decay = jnp.exp(log_gamma[None, :] * (steps[:, None] + 1.0))
    k_decay = jnp.exp(log_gamma[None, :] * (count - 1.0 - steps[:, None]))
    block_decay = jnp.exp(log_gamma * count)
    return (intra, q_decay, k_decay, block_decay)


def rotate(values, offset):
    half_dim = values.shape[-1] // 2
    freqs = jnp.power(
        ROTARY_BASE, -jnp.arange(half_dim, dtype=jnp.float32) * (2.0 / values.shape[-1])
    )
    places = (offset + jnp.arange(values.shape[1])).astype(jnp.float32)
    angles = places[:, None] * freqs[None, :]
    cosine = jnp.cos(angles)[None, :, None, :]
    sine = jnp.sin(angles)[None, :, None, :]
    first = values[..., :half_dim]
    second = values[..., half_dim:]
    return jnp.concatenate(
        [first * cosine - second * sine, second * cosine + first * sine], axis=-1
    )


def plain_local(
    stream_in,
    state_in,
    norm_gain,
    query_weight,
    key_weight,
    value_weight,
    gate_weight,
    group_gain,
    output_weight,
):
    seqs, new_tok, width = stream_in.shape
    heads, local_dim = (value_weight.shape[2], value_weight.shape[3])
    head_dim = HEAD_DIM
    log_gamma = log_decays(heads)
    intra, q_decay, k_decay, block_decay = decay_tables(log_gamma, new_tok)
    highest = lax.Precision.HIGHEST
    share_cols = width // lax.axis_size("tp")
    col_start = lax.axis_index("tp") * share_cols
    layers = state_in.shape[0]
    stream = stream_in
    stream_share = stream_in
    new_states = []
    for layer_no in range(layers):
        stream_f = stream.astype(jnp.float32)
        normed = stream_f * lax.rsqrt(
            jnp.mean(stream_f * stream_f, axis=-1, keepdims=True) + EPS_RMS
        )
        normed = (normed * norm_gain[layer_no].astype(jnp.float32)).astype(jnp.bfloat16)
        flat = normed.reshape(seqs * new_tok, width)
        query_part = jnp.dot(flat, query_weight[layer_no], preferred_element_type=jnp.float32)
        query_part = query_part.astype(jnp.bfloat16).reshape(seqs, new_tok, -1)
        key_part = jnp.dot(flat, key_weight[layer_no], preferred_element_type=jnp.float32)
        key_part = key_part.astype(jnp.bfloat16).reshape(seqs, new_tok, -1)

        def project_local(weight):
            result = jnp.dot(
                flat, weight.reshape(width, heads * local_dim), preferred_element_type=jnp.float32
            )
            result = lax.optimization_barrier(result.astype(jnp.bfloat16))
            return result.astype(jnp.float32).reshape(seqs, new_tok, heads, local_dim)

        values_f = project_local(value_weight[layer_no])
        gates_f = project_local(gate_weight[layer_no])
        queries, key_rows = (
            lax.all_gather(query_part, "tp", axis=2, tiled=True),
            lax.all_gather(key_part, "tp", axis=2, tiled=True),
        )
        queries = queries.astype(jnp.float32).reshape(seqs, new_tok, heads, head_dim)
        key_rows = key_rows.astype(jnp.float32).reshape(seqs, new_tok, heads, head_dim)
        rot_q = rotate(queries, PAST)
        rot_k = rotate(key_rows, PAST) * head_dim ** (-0.5)
        scores = jnp.einsum("bthd,bshd->bhts", rot_q, rot_k, precision=highest) * intra[None]
        inner = jnp.einsum("bhts,bshe->bthe", scores, values_f, precision=highest)
        state = state_in[layer_no]
        carried = (
            jnp.einsum("bthd,bhed->bthe", rot_q, state, precision=highest)
            * q_decay[None, :, :, None]
        )
        mixed = inner + carried
        new_state = state * block_decay[None, :, None, None] + jnp.einsum(
            "bthe,bthd->bhed", values_f, rot_k * k_decay[None, :, :, None], precision=highest
        )
        new_states.append(new_state)
        totals, squares = lax.psum((jnp.sum(mixed, axis=-1), jnp.sum(mixed * mixed, axis=-1)), "tp")
        mean_o = (totals / head_dim)[..., None]
        var_o = (squares / head_dim)[..., None] - mean_o * mean_o
        normal = (
            (mixed - mean_o)
            * lax.rsqrt(var_o + EPS_GROUP)
            * group_gain[layer_no].astype(jnp.float32)[None, None]
        )
        gated = (jax.nn.silu(gates_f) * normal).astype(jnp.bfloat16)
        partial_out = jnp.dot(
            gated.reshape(seqs * new_tok, heads * local_dim),
            output_weight[layer_no].reshape(heads * local_dim, width),
            preferred_element_type=jnp.float32,
        ).reshape(seqs, new_tok, width)
        share_out = lax.psum_scatter(partial_out, "tp", scatter_dimension=2, tiled=True)
        own_cols = lax.dynamic_slice_in_dim(stream, col_start, share_cols, 2)
        stream_share = (own_cols.astype(jnp.float32) + share_out).astype(jnp.bfloat16)
        if layer_no + 1 < layers:
            stream = lax.all_gather(stream_share, "tp", axis=2, tiled=True)
    result = stream_share
    return (result, jnp.stack(new_states))


LAG = 0
F32 = jnp.float32
BF16 = jnp.bfloat16


def nt_dot(a, b, precision=None):
    return lax.dot_general(
        a, b, (((1,), (1,)), ((), ())), preferred_element_type=F32, precision=precision
    )


def log2(value):
    return int(value).bit_length() - 1


def rotary_tables(heads, new_tok, head_dim):
    half = head_dim // 2
    freqs = np.power(
        np.float32(ROTARY_BASE), -np.arange(half, dtype=np.float32) * np.float32(2.0 / head_dim)
    ).astype(np.float32)
    tok = np.arange(8) % new_tok
    places = (PAST + tok).astype(np.float32)
    angles = (places[:, None] * freqs[None, :]).astype(np.float32).astype(np.float64)
    gamma = 1.0 - np.power(2.0, -5.0 - np.arange(heads))
    grow = np.power(gamma[:, None], tok[None, :] + 1.0)[:, :, None]
    shrink = head_dim ** (-0.5) / grow
    cosine, sine = np.cos(angles)[None], np.sin(angles)[None]
    block = np.broadcast_to(np.power(gamma, new_tok)[:, None, None], (heads, 8, half))
    return np.stack(
        [cosine * grow, sine * grow, cosine * shrink, sine * shrink, block]
    ).astype(np.float32)


def kernel(
    n, head_dim, groups, lag,
    x_hbm, st_hbm, ng_ref, qw_hbm, kw_hbm, vw_hbm, gw_hbm, gg_ref, ow_hbm, tab_ref,
    y_ref, stv,
    xs, nv, wqk, wvg, wo, qkg, kh, vts, sb, pbs, pbr, yss, ysr, rss, rsr, mkc, mks, fold,
    lsem, ag_s, ag_r, st_s, st_r, pb_s, pb_r, ys_s, ys_r, rs_s, rs_r,
):
    layers, seqs, heads, e_dim, _ = st_hbm.shape
    tok = x_hbm.shape[0] // seqs
    width = x_hbm.shape[1]
    seqs = seqs // groups
    rows = seqs * tok
    share = width // n
    cols = qw_hbm.shape[2]
    he = heads * e_dim
    half = head_dim // 2
    nc = n // 2
    me = lax.axis_index("tp")
    core = lax.rem(me, 2)
    chip = lax.div(me, 2)
    partner = chip * 2 + 1 - core

    nz = nc // 2
    yy = lax.rem(chip, 2)
    zz = lax.div(chip, 2)

    def at_z(o, y, c):
        z, bit = zz, 1
        while bit < nz:
            if o & bit:
                z = z + bit - 2 * bit * lax.rem(lax.div(z, bit), 2)
            bit = 2 * bit
        return (z * 2 + y) * 2 + c

    facing = at_z(0, 1 - yy, core)
    far = list(range(2, nz)) + [1]

    def remote(src, dst, ssem, rsem, device):
        return pltpu.make_async_remote_copy(
            src_ref=src, dst_ref=dst, send_sem=ssem, recv_sem=rsem,
            device_id={"tp": device}, device_id_type=pl.DeviceIdType.MESH,
        )

    loads = {}
    count = 0

    def load(name, src, dst):
        nonlocal count
        loads[name] = pltpu.make_async_copy(src, dst, lsem.at[count])
        loads[name].start()
        count += 1

    for g in range(groups):
        for j in range(n):
            source = x_hbm.at[pl.ds(g * rows, rows), pl.ds(j * share, share)]
            load(("x", g, j), source, xs.at[g, j])
    for l in range(layers):
        load(("q", l), qw_hbm.at[l], wqk.at[l, :, pl.ds(0, cols)])
        load(("k", l), kw_hbm.at[l], wqk.at[l, :, pl.ds(cols, cols)])
        load(("v", l), vw_hbm.at[l], wvg.at[l, pl.ds(0, he)])
        load(("g", l), gw_hbm.at[l], wvg.at[l, pl.ds(he, he)])
        load(("s", l), st_hbm.at[l], stv.at[l])
        load(("o", l), ow_hbm.at[l], wo.at[l])

    barrier = pltpu.get_barrier_semaphore()
    for o in range(1, n):
        pl.semaphore_signal(
            barrier, inc=1, device_id={"tp": lax.rem(me + o, n)},
            device_id_type=pl.DeviceIdType.MESH,
        )

    be = seqs * e_dim

    def iota(shape, dim, shift=0):
        return jnp.right_shift(lax.broadcasted_iota(jnp.int32, shape, dim), shift)

    te, tt = log2(e_dim), log2(tok)
    mkc[...] = (iota((rows, be), 0, tt) == iota((rows, be), 1, te)).astype(F32).astype(BF16)
    mks[...] = (iota((be, rows), 0, te) == iota((be, rows), 1, tt)).astype(F32).astype(BF16)
    low = e_dim - 1
    fold[...] = (
        jnp.bitwise_and(iota((be, he), 0), low) == jnp.bitwise_and(iota((be, he), 1), low)
    ).astype(F32).astype(BF16)
    causal = (
        (iota((rows, rows), 0, tt) == iota((rows, rows), 1, tt))
        & (iota((rows, rows), 0) >= iota((rows, rows), 1))
    ).astype(F32)
    heads_of = (iota((heads, he), 0) == iota((heads, he), 1, te)).astype(F32)
    place = (
        iota((e_dim, he), 0) == jnp.bitwise_and(iota((e_dim, he), 1), low)
    ).astype(F32)
    highest = lax.Precision.HIGHEST

    def gather_start(buf, p):
        own = buf.at[me]
        sent = [remote(own, own, ag_s.at[p, nz], ag_r.at[p, nz], facing)]
        for o in far:
            sent.append(remote(own, own, ag_s.at[p, o], ag_r.at[p, o], at_z(o, yy, core)))
        sent.append(remote(own, own, ag_s.at[p, nc], ag_r.at[p, nc], partner))
        for copy in sent:
            copy.start()
        return sent

    def gather_finish(buf, p, sent):
        def arrive(slot, k):
            remote(slot, slot, ag_s.at[p, k], ag_r.at[p, k], partner).wait_recv()

        def forward(slot, k, device):
            copy = remote(slot, slot, ag_s.at[p, k], ag_r.at[p, k], device)
            copy.start()
            sent.append(copy)

        for o in range(1, nz):
            slot = buf.at[at_z(o, yy, core)]
            arrive(slot, o)
            forward(slot, nz + o, facing)
            forward(slot, nc + o, partner)
        yield
        for o in range(nz):
            slot = buf.at[at_z(o, 1 - yy, core)]
            arrive(slot, nz + o)
            forward(slot, nc + nz + o, partner)
        yield
        for o in range(nz):
            arrive(buf.at[at_z(o, yy, 1 - core)], nc + o)
            arrive(buf.at[at_z(o, 1 - yy, 1 - core)], nc + nz + o)

    def spread(table):
        return jnp.broadcast_to(table[None], (rows // 8, 8, half)).reshape(rows, half)

    started = []
    waited = set()

    def once(key):
        if key not in waited:
            waited.add(key)
            loads[key].wait()

    def chain(g):
        mine = pl.ds(g * seqs, seqs)
        for l in range(layers):
            lg = l * groups + g
            if l == 0:
                for j in range(n):
                    loads[("x", g, j)].wait()

            def square(j, acc):
                block = xs[lg, j].astype(F32)
                return acc + block * block

            total = lax.fori_loop(0, n, square, jnp.zeros((rows, share), F32))
            scale = lax.rsqrt(jnp.sum(total, axis=1, keepdims=True) / width + EPS_RMS)

            def normalise(j, carry):
                at = pl.ds(pl.multiple_of(j * share, share), share)
                gain = ng_ref[l : l + 1, at].astype(F32)
                nv[g, :, at] = (xs[lg, j].astype(F32) * scale * gain).astype(BF16)
                return carry

            lax.fori_loop(0, n, normalise, 0)
            once(("q", l))
            once(("k", l))
            qkg[lg, me] = jnp.dot(nv[g], wqk[l], preferred_element_type=F32).astype(BF16)
            if l == 0 and g == 0:
                pl.semaphore_wait(barrier, n - 1)
            sent = gather_start(qkg.at[lg], lg)
            once(("v", l))
            once(("g", l))
            vg = nt_dot(nv[g], wvg[l])
            values = vg[:, :he].astype(BF16)
            gates = vg[:, he:].astype(BF16).astype(F32)
            vts[g] = jnp.transpose(values.astype(F32)).astype(BF16)
            once(("s", l))
            yield
            yield from gather_finish(qkg.at[lg], lg, sent)
            started.extend(sent)

            def mix(h, acc):
                qk_a = qkg[lg, 2 * h].astype(F32)
                qk_b = qkg[lg, 2 * h + 1].astype(F32)
                qa, ka = qk_a[:, :half], qk_a[:, half:]
                qb, kb = qk_b[:, :half], qk_b[:, half:]
                cq, sq = spread(tab_ref[0, h]), spread(tab_ref[1, h])
                ck, sk = spread(tab_ref[2, h]), spread(tab_ref[3, h])
                rq = jnp.concatenate([qa * cq - qb * sq, qb * cq + qa * sq], axis=1).astype(BF16)
                rk = jnp.concatenate([ka * ck - kb * sk, kb * ck + ka * sk], axis=1).astype(BF16)
                kh[g * heads + h] = rk
                state = stv[l, mine, h].reshape(be, head_dim).astype(BF16)
                scores = (nt_dot(rq, rk) * causal).astype(BF16)
                carried = nt_dot(rq, state).astype(BF16) * mkc[...]
                part = jnp.dot(scores, values, preferred_element_type=F32)
                part = part + jnp.dot(carried, fold[...], preferred_element_type=F32)
                own = (iota((1, he), 1, te) == h).astype(F32)
                return acc + part * own

            mixed = lax.fori_loop(0, heads, mix, jnp.zeros((rows, he), F32), unroll=True)
            sums = nt_dot(heads_of, mixed, highest)
            squares = nt_dot(heads_of, mixed * mixed, highest)
            sb[lg, me] = jnp.concatenate([sums, squares], axis=1)
            sent = []
            for o in range(1, n):
                sent.append(
                    remote(sb.at[lg, me], sb.at[lg, me], st_s.at[lg, o], st_r.at[lg, o], lax.rem(me + o, n))
                )
            for copy in sent:
                copy.start()
            started.extend(sent)

            def update(h, carry):
                at = pl.ds(pl.multiple_of(h * e_dim, e_dim), e_dim)
                tall = jnp.broadcast_to(vts[g, at, :][None], (seqs, e_dim, rows)).reshape(be, rows)
                fresh = jnp.dot(tall * mks[...], kh[g * heads + h], preferred_element_type=F32)
                row = tab_ref[4, h][0:1, :]
                fade = jnp.concatenate([row, row], axis=1)
                state = stv[l, mine, h].reshape(be, head_dim)
                stv[l, mine, h] = ((state + fresh) * fade).reshape(seqs, e_dim, head_dim)
                return carry

            lax.fori_loop(0, heads, update, 0, unroll=True)
            yield

            for o in range(1, n):
                slot = sb.at[lg, lax.rem(me - o + n, n)]
                remote(slot, slot, st_s.at[lg, o], st_r.at[lg, o], partner).wait_recv()
            stats = jnp.sum(sb[lg], axis=0)
            mean = stats[:, :rows] / head_dim
            var = stats[:, rows:] / head_dim - mean * mean
            rstd = lax.rsqrt(var + EPS_GROUP)

            def expand(small):
                return lax.dot_general(
                    small, heads_of, (((0,), (0,)), ((), ())),
                    preferred_element_type=F32, precision=highest,
                )

            gain = jnp.dot(gg_ref[l].astype(F32), place, preferred_element_type=F32, precision=highest)
            gain = jnp.sum(gain * heads_of, axis=0, keepdims=True)
            normal = (mixed - expand(mean)) * expand(rstd) * gain
            gated = (gates / (1.0 + jnp.exp(-gates)) * normal).astype(BF16)

            once(("o", l))

            def chunk(j):
                at = pl.ds(pl.multiple_of(j * share, share), share)
                return jnp.dot(gated, wo[l, :, at], preferred_element_type=F32)

            order = far + [0]
            for side in (1, 0):
                for o in order:
                    k = side * nz + o
                    y = 1 - yy if side else yy
                    pbs[lg, k] = chunk(at_z(o, y, 1 - core)).astype(BF16)
                    copy = remote(pbs.at[lg, k], pbr.at[lg, k], pb_s.at[lg, k], pb_r.at[lg, k], partner)
                    copy.start()
                    started.append(copy)

            yield

            def paired(o, side):
                k = side * nz + o
                own = chunk(at_z(o, 1 - yy if side else yy, core))
                remote(pbs.at[lg, k], pbr.at[lg, k], pb_s.at[lg, k], pb_r.at[lg, k], partner).wait_recv()
                return own + pbr[lg, k].astype(F32)

            for o in order:
                yss[lg, o] = paired(o, 1).astype(BF16)
                copy = remote(yss.at[lg, o], ysr.at[lg, o], ys_s.at[lg, o], ys_r.at[lg, o], facing)
                copy.start()
                started.append(copy)
            yield
            acc = None
            for o in order:
                own = paired(o, 0)
                remote(yss.at[lg, o], ysr.at[lg, o], ys_s.at[lg, o], ys_r.at[lg, o], facing).wait_recv()
                own = own + ysr[lg, o].astype(F32)
                if o:
                    rss[lg, o] = own.astype(BF16)
                    copy = remote(
                        rss.at[lg, o], rsr.at[lg, o], rs_s.at[lg, o], rs_r.at[lg, o], at_z(o, yy, core)
                    )
                    copy.start()
                    started.append(copy)
                else:
                    acc = own
            yield
            for o in range(1, nz):
                remote(rss.at[lg, o], rsr.at[lg, o], rs_s.at[lg, o], rs_r.at[lg, o], facing).wait_recv()
                acc = acc + rsr[lg, o].astype(F32)
            fresh_x = (xs[lg, me].astype(F32) + acc).astype(BF16)
            if l + 1 < layers:
                xs[lg + groups, me] = fresh_x
                sent = gather_start(xs.at[lg + groups], layers * groups + lg)
                yield
                yield from gather_finish(xs.at[lg + groups], layers * groups + lg, sent)
                started.extend(sent)
            else:
                y_ref[pl.ds(g * rows, rows), :] = fresh_x

    chains = [chain(g) for g in range(groups)]
    live = list(range(groups))
    step = 0
    while live:
        for g in list(live):
            if step >= lag * g and next(chains[g], live) is live:
                live.remove(g)
        step += 1
    for copy in started:
        copy.wait_send()


def store_kernel(y_ref, state_ref, y_out, state_out, sem):
    copies = [
        pltpu.make_async_copy(state_ref.at[l], state_out.at[l], sem.at[l])
        for l in range(state_ref.shape[0])
    ]
    for copy in copies:
        copy.start()
    y_out[...] = y_ref[...]
    for copy in copies:
        copy.wait()


def local(
    stream_in, state_in, norm_gain, query_weight, key_weight,
    value_weight, gate_weight, group_gain, output_weight,
):
    n = lax.axis_size("tp")
    seqs, tok, width = stream_in.shape
    layers, _, heads, e_dim, head_dim = state_in.shape
    cols = query_weight.shape[2]
    rows = seqs * tok
    he = heads * e_dim
    share = width // n
    fits = (
        cols == 128 and head_dim == 256 and he == 128 and heads == 8 and e_dim == 16
        and share % 128 == 0 and n % 4 == 0 and n & (n - 1) == 0 and rows == 128 and 8 % tok == 0
    )
    if not fits:
        return plain_local(
            stream_in, state_in, norm_gain, query_weight, key_weight,
            value_weight, gate_weight, group_gain, output_weight,
        )
    groups = 1
    nc = n // 2
    part = rows // groups
    be = seqs * e_dim // groups
    steps = layers * groups
    hbm = pl.BlockSpec(memory_space=pl.ANY)
    vmem = pl.BlockSpec(memory_space=pltpu.VMEM)
    dma = pltpu.SemaphoreType.DMA
    tables = jnp.asarray(rotary_tables(heads, tok, head_dim))
    flat = lambda w: jnp.transpose(w, (0, 2, 3, 1)).reshape(layers, he, width)
    y, new_state = pl.pallas_call(
        functools.partial(kernel, n, head_dim, groups, LAG),
        name="retention",
        out_shape=(
            jax.ShapeDtypeStruct((rows, share), BF16),
            pltpu.VMEM(state_in.shape, F32),
        ),
        in_specs=[hbm, hbm, vmem, hbm, hbm, hbm, hbm, vmem, hbm, vmem],
        out_specs=(vmem, vmem),
        scratch_shapes=[
            pltpu.VMEM((steps, n, part, share), BF16),
            pltpu.VMEM((groups, part, width), BF16),
            pltpu.VMEM((layers, width, 2 * cols), BF16),
            pltpu.VMEM((layers, 2 * he, width), BF16),
            pltpu.VMEM((layers, he, width), BF16),
            pltpu.VMEM((steps, n, part, 2 * cols), BF16),
            pltpu.VMEM((groups * heads, part, head_dim), BF16),
            pltpu.VMEM((groups, he, part), BF16),
            pltpu.VMEM((steps, n, heads, 2 * part), F32),
            pltpu.VMEM((steps, nc, part, share), BF16),
            pltpu.VMEM((steps, nc, part, share), BF16),
            pltpu.VMEM((steps, nc // 2, part, share), BF16),
            pltpu.VMEM((steps, nc // 2, part, share), BF16),
            pltpu.VMEM((steps, nc // 2, part, share), BF16),
            pltpu.VMEM((steps, nc // 2, part, share), BF16),
            pltpu.VMEM((part, be), BF16),
            pltpu.VMEM((be, part), BF16),
            pltpu.VMEM((be, he), BF16),
            dma((groups * n + 6 * layers,)),
            dma((2 * steps, n)),
            dma((2 * steps, n)),
            dma((steps, n)),
            dma((steps, n)),
            dma((steps, nc)),
            dma((steps, nc)),
            dma((steps, nc // 2)),
            dma((steps, nc // 2)),
            dma((steps, nc // 2)),
            dma((steps, nc // 2)),
        ],
        compiler_params=pltpu.CompilerParams(
            collective_id=0, has_side_effects=True, vmem_limit_bytes=44 * 2**20
        ),
    )(
        stream_in.reshape(rows, width), state_in, norm_gain, query_weight, key_weight,
        flat(value_weight), flat(gate_weight), group_gain,
        output_weight.reshape(layers, he, width), tables,
    )
    y, new_state = pl.pallas_call(
        store_kernel,
        name="store",
        out_shape=(
            jax.ShapeDtypeStruct((rows, share), BF16),
            jax.ShapeDtypeStruct(state_in.shape, F32),
        ),
        in_specs=[vmem, hbm],
        out_specs=(vmem, hbm),
        scratch_shapes=[dma((layers,))],
        compiler_params=pltpu.CompilerParams(vmem_limit_bytes=2 * 2**20),
    )(y, new_state)
    return y.reshape(seqs, tok, share), new_state


def solution(mesh):
    in_specs = (
        P("grp", None, None),
        P(None, "grp", None, "tp", None),
        P(),
        P(None, None, "tp"),
        P(None, None, "tp"),
        P(None, None, None, "tp"),
        P(None, None, None, "tp"),
        P(None, None, "tp"),
        P(None, None, "tp", None),
    )
    out_specs = (P("grp", None, "tp"), P(None, "grp", None, "tp", None))
    return jax.shard_map(local, mesh=mesh, in_specs=in_specs, out_specs=out_specs, check_vma=False)
```

profile of v0, /device:TPU:0, one launch (start us, length us, event | category | flops | bytes accessed | tf_op | source)
XLA Modules:
  0.0 91.9 jit_solution(18214433493446871272)
XLA Ops:
  0.6 0.0 copy-start
  0.6 0.0 copy-start.2
  0.7 0.0 copy-start.1
  0.7 1.4 %reshape.19.x_hbm = bf16[128,4096]{1,0:T(8,128)(2,1)S(1)} reshape(bf16[32,4,4096]{2,1,0:T(4,128)(2,1)} %param.10) | data formatting | bytes 2097152 | tf_op jit(solution)/shard_map/reshape | solution.py:568
  2.1 0.0 copy-done
  2.1 0.0 copy-done.2
  2.1 0.0 copy-done.1
  2.1 85.8 %retention.1 = (bf16[128,256]{1,0:T(8,128)(2,1)S(1)}, f32[2,32,8,16,256]{4,3,2,1,0:T(8,128)S(1)}) custom-call(bf16[128,4096]{1,0:T(8,128)(2,1)S(1)} %reshape.19.x_hbm, f32[2,32,8,16,256]{4,3,2,1,0:T(8,128)} %st_hbm.1, bf16[2,4096]{1,0:T(2,128)(2,1)S(1)} %copy-done.1, bf16[2,4096,128]{2,1,0:T(8,128)(2,1)} %qw_hbm.1, bf16[2,4096,128]{2,1,0:T(8,128)(2,1)} %kw_hbm.1, ...), custom_call_target="tpu_custom_call" | custom-call | tf_op jit(solution)/shard_map/retention/pallas_call | solution.py:524
  87.9 3.4 %store.1 = (bf16[128,256]{1,0:T(8,128)(2,1)S(1)}, f32[2,32,8,16,256]{4,3,2,1,0:T(8,128)}) custom-call(bf16[128,256]{1,0:T(8,128)(2,1)S(1)} %get-tuple-element.6.y_ref, f32[2,32,8,16,256]{4,3,2,1,0:T(8,128)S(1)} %get-tuple-element.7.state_ref), custom_call_target="tpu_custom_call" | custom-call | tf_op jit(solution)/shard_map/store/pallas_call | solution.py:572
  91.3 0.7 reshape.23
Async XLA Ops:
  0.6 1.4 %copy-start = (f32[5,8,8,128]{3,2,1,0:T(8,128)S(1)}, f32[5,8,8,128]{3,2,1,0:T(8,128)}, u32[]{:S(2)}) copy-start(f32[5,8,8,128]{3,2,1,0:T(8,128)} %constant.2.clone.tab_ref) | copy-start | bytes 491524
  0.6 1.4 %copy-start.2 = (bf16[2,8,16]{2,1,0:T(8,128)(2,1)S(1)}, bf16[2,8,16]{2,1,0:T(8,128)(2,1)}, u32[]{:S(2)}) copy-start(bf16[2,8,16]{2,1,0:T(8,128)(2,1)} %gg_ref.1) | copy-start | bytes 1540
  0.7 1.4 %copy-start.1 = (bf16[2,4096]{1,0:T(2,128)(2,1)S(1)}, bf16[2,4096]{1,0:T(2,128)(2,1)}, u32[]{:S(2)}) copy-start(bf16[2,4096]{1,0:T(2,128)(2,1)} %ng_ref.1) | copy-start | bytes 49156
where the time goes:
time: 92.1 us; the launch traced here: 91.9 us
  Pallas kernels  89.2 us (97%)
  local copies, waits for them, and re-layouts  2.06 us (2%)
    pallas_call x1, Pallas kernels, local(): pl.pallas_call(functools.partial(kernel, n, head_dim, groups, LAG), name=...  85.8 us
    pallas_call x1, Pallas kernels, local(): pl.pallas_call(store_kernel, name='store', out_shape=(jax.ShapeDtypeStruc...  3.41 us

commit v1 on v0

v1 whole, which is shorter than its diff:
```python
import functools

import jax
import jax.numpy as jnp
import numpy as np
from jax import lax
from jax.experimental import pallas as pl
from jax.experimental.pallas import tpu as pltpu
from jax.sharding import PartitionSpec as P

HEAD_DIM = 256
PAST = 1024


EPS_RMS = 1e-06
EPS_GROUP = 1e-05
ROTARY_BASE = 10000.0


def log_decays(count):
    return jnp.log(1.0 - jnp.power(2.0, -5.0 - jnp.arange(count, dtype=jnp.float32)))


def decay_tables(log_gamma, count):
    steps = jnp.arange(count, dtype=jnp.float32)
    gap = steps[:, None] - steps[None, :]
    intra = jnp.where(
        gap[None] >= 0, jnp.exp(log_gamma[:, None, None] * jnp.maximum(gap, 0.0)[None]), 0.0
    )
    q_decay = jnp.exp(log_gamma[None, :] * (steps[:, None] + 1.0))
    k_decay = jnp.exp(log_gamma[None, :] * (count - 1.0 - steps[:, None]))
    block_decay = jnp.exp(log_gamma * count)
    return (intra, q_decay, k_decay, block_decay)


def rotate(values, offset):
    half_dim = values.shape[-1] // 2
    freqs = jnp.power(
        ROTARY_BASE, -jnp.arange(half_dim, dtype=jnp.float32) * (2.0 / values.shape[-1])
    )
    places = (offset + jnp.arange(values.shape[1])).astype(jnp.float32)
    angles = places[:, None] * freqs[None, :]
    cosine = jnp.cos(angles)[None, :, None, :]
    sine = jnp.sin(angles)[None, :, None, :]
    first = values[..., :half_dim]
    second = values[..., half_dim:]
    return jnp.concatenate(
        [first * cosine - second * sine, second * cosine + first * sine], axis=-1
    )


def plain_local(
    stream_in,
    state_in,
    norm_gain,
    query_weight,
    key_weight,
    value_weight,
    gate_weight,
    group_gain,
    output_weight,
):
    seqs, new_tok, width = stream_in.shape
    heads, local_dim = (value_weight.shape[2], value_weight.shape[3])
    head_dim = HEAD_DIM
    log_gamma = log_decays(heads)
    intra, q_decay, k_decay, block_decay = decay_tables(log_gamma, new_tok)
    highest = lax.Precision.HIGHEST
    share_cols = width // lax.axis_size("tp")
    col_start = lax.axis_index("tp") * share_cols
    layers = state_in.shape[0]
    stream = stream_in
    stream_share = stream_in
    new_states = []
    for layer_no in range(layers):
        stream_f = stream.astype(jnp.float32)
        normed = stream_f * lax.rsqrt(
            jnp.mean(stream_f * stream_f, axis=-1, keepdims=True) + EPS_RMS
        )
        normed = (normed * norm_gain[layer_no].astype(jnp.float32)).astype(jnp.bfloat16)
        flat = normed.reshape(seqs * new_tok, width)
        query_part = jnp.dot(flat, query_weight[layer_no], preferred_element_type=jnp.float32)
        query_part = query_part.astype(jnp.bfloat16).reshape(seqs, new_tok, -1)
        key_part = jnp.dot(flat, key_weight[layer_no], preferred_element_type=jnp.float32)
        key_part = key_part.astype(jnp.bfloat16).reshape(seqs, new_tok, -1)

        def project_local(weight):
            result = jnp.dot(
                flat, weight.reshape(width, heads * local_dim), preferred_element_type=jnp.float32
            )
            result = lax.optimization_barrier(result.astype(jnp.bfloat16))
            return result.astype(jnp.float32).reshape(seqs, new_tok, heads, local_dim)

        values_f = project_local(value_weight[layer_no])
        gates_f = project_local(gate_weight[layer_no])
        queries, key_rows = (
            lax.all_gather(query_part, "tp", axis=2, tiled=True),
            lax.all_gather(key_part, "tp", axis=2, tiled=True),
        )
        queries = queries.astype(jnp.float32).reshape(seqs, new_tok, heads, head_dim)
        key_rows = key_rows.astype(jnp.float32).reshape(seqs, new_tok, heads, head_dim)
        rot_q = rotate(queries, PAST)
        rot_k = rotate(key_rows, PAST) * head_dim ** (-0.5)
        scores = jnp.einsum("bthd,bshd->bhts", rot_q, rot_k, precision=highest) * intra[None]
        inner = jnp.einsum("bhts,bshe->bthe", scores, values_f, precision=highest)
        state = state_in[layer_no]
        carried = (
            jnp.einsum("bthd,bhed->bthe", rot_q, state, precision=highest)
            * q_decay[None, :, :, None]
        )
        mixed = inner + carried
        new_state = state * block_decay[None, :, None, None] + jnp.einsum(
            "bthe,bthd->bhed", values_f, rot_k * k_decay[None, :, :, None], precision=highest
        )
        new_states.append(new_state)
        totals, squares = lax.psum((jnp.sum(mixed, axis=-1), jnp.sum(mixed * mixed, axis=-1)), "tp")
        mean_o = (totals / head_dim)[..., None]
        var_o = (squares / head_dim)[..., None] - mean_o * mean_o
        normal = (
            (mixed - mean_o)
            * lax.rsqrt(var_o + EPS_GROUP)
            * group_gain[layer_no].astype(jnp.float32)[None, None]
        )
        gated = (jax.nn.silu(gates_f) * normal).astype(jnp.bfloat16)
        partial_out = jnp.dot(
            gated.reshape(seqs * new_tok, heads * local_dim),
            output_weight[layer_no].reshape(heads * local_dim, width),
            preferred_element_type=jnp.float32,
        ).reshape(seqs, new_tok, width)
        share_out = lax.psum_scatter(partial_out, "tp", scatter_dimension=2, tiled=True)
        own_cols = lax.dynamic_slice_in_dim(stream, col_start, share_cols, 2)
        stream_share = (own_cols.astype(jnp.float32) + share_out).astype(jnp.bfloat16)
        if layer_no + 1 < layers:
            stream = lax.all_gather(stream_share, "tp", axis=2, tiled=True)
    result = stream_share
    return (result, jnp.stack(new_states))


F32 = jnp.float32
BF16 = jnp.bfloat16
XPARTS = 4
scope = jax.named_scope


def nt_dot(a, b, precision=None):
    return lax.dot_general(
        a, b, (((1,), (1,)), ((), ())), preferred_element_type=F32, precision=precision
    )


def log2(value):
    return int(value).bit_length() - 1


def rotary_tables(heads, new_tok, head_dim):
    half = head_dim // 2
    freqs = np.power(
        np.float32(ROTARY_BASE), -np.arange(half, dtype=np.float32) * np.float32(2.0 / head_dim)
    ).astype(np.float32)
    tok = np.arange(8) % new_tok
    places = (PAST + tok).astype(np.float32)
    angles = (places[:, None] * freqs[None, :]).astype(np.float32).astype(np.float64)
    gamma = 1.0 - np.power(2.0, -5.0 - np.arange(heads))
    grow = np.power(gamma[:, None], tok[None, :] + 1.0)[:, :, None]
    shrink = head_dim ** (-0.5) / grow
    cosine, sine = np.cos(angles)[None], np.sin(angles)[None]
    block = np.broadcast_to(np.power(gamma, new_tok)[:, None, None], (heads, 8, half))
    return np.stack(
        [cosine * grow, sine * grow, cosine * shrink, sine * shrink, block]
    ).astype(np.float32)


def kernel(
    n, head_dim,
    x_hbm, st_hbm, ng_hbm, qw_hbm, kw_hbm, vw_hbm, gw_hbm, gg_hbm, ow_hbm, tab_hbm,
    y_ref, stv,
    ng_ref, gg_ref, tab_ref, xr, xs, nv, wqk, wvg, wo, qkg, kh, vts, sb, pbs, pbr, yss, ysr, rss, rsr, mkc, mks, fold, sqa, qka,
    lsem, ag_s, st_s, rs_s, aq_r, ax_r, st_r, pb_r, ys_r, rs_r,
):
    layers, seqs, heads, e_dim, _ = st_hbm.shape
    tok = x_hbm.shape[1]
    width = x_hbm.shape[2]
    rows = seqs * tok
    share = width // n
    cols = qw_hbm.shape[2]
    he = heads * e_dim
    half = head_dim // 2
    nc = n // 2
    me = lax.axis_index("tp")
    core = lax.rem(me, 2)
    chip = lax.div(me, 2)
    partner = chip * 2 + 1 - core

    nz = nc // 2
    yy = lax.rem(chip, 2)
    zz = lax.div(chip, 2)

    def chip_at(o, y):
        z, bit = zz, 1
        while bit < nz:
            if o & bit:
                z = z + bit - 2 * bit * lax.rem(lax.div(z, bit), 2)
            bit = 2 * bit
        return z * 2 + y

    def at_z(o, y, c):
        return chip_at(o, y) * 2 + c

    facing = at_z(0, 1 - yy, core)
    far = list(range(2, nz)) + [1]
    near = [1] + list(range(nz - 1, 1, -1))

    def remote(src, dst, ssem, rsem, device):
        return pltpu.make_async_remote_copy(
            src_ref=src, dst_ref=dst, send_sem=ssem, recv_sem=rsem,
            device_id={"tp": device}, device_id_type=pl.DeviceIdType.MESH,
        )

    loads = {}
    count = 0

    def load(name, src, dst):
        nonlocal count
        loads[name] = pltpu.make_async_copy(src, dst, lsem.at[count])
        loads[name].start()
        count += 1

    wide = width // XPARTS
    for j in range(XPARTS):
        at = pl.ds(j * wide, wide)
        load(("x", j), x_hbm.at[:, :, at], xr.at[:, :, at])
    load("ng", ng_hbm, ng_ref)

    barrier = pltpu.get_barrier_semaphore()
    for o in range(1, n):
        pl.semaphore_signal(
            barrier, inc=1, device_id={"tp": lax.rem(me + o, n)},
            device_id_type=pl.DeviceIdType.MESH,
        )

    for l in range(layers):
        load(("q", l), qw_hbm.at[l], wqk.at[l, :, pl.ds(0, cols)])
        load(("k", l), kw_hbm.at[l], wqk.at[l, :, pl.ds(cols, cols)])
        load(("v", l), vw_hbm.at[l], wvg.at[l, pl.ds(0, he)])
        load(("g", l), gw_hbm.at[l], wvg.at[l, pl.ds(he, he)])
        load(("s", l), st_hbm.at[l], stv.at[l])
        load(("o", l), ow_hbm.at[l], wo.at[l])
        if l == 0:
            load("tab", tab_hbm, tab_ref)
            load("gg", gg_hbm, gg_ref)

    be = seqs * e_dim

    def iota(shape, dim, shift=0):
        return jnp.right_shift(lax.broadcasted_iota(jnp.int32, shape, dim), shift)

    te, tt = log2(e_dim), log2(tok)
    low = e_dim - 1
    causal = (
        (iota((rows, rows), 0, tt) == iota((rows, rows), 1, tt))
        & (iota((rows, rows), 0) >= iota((rows, rows), 1))
    ).astype(F32)
    heads_of = (iota((heads, he), 0) == iota((heads, he), 1, te)).astype(F32)
    place = (
        iota((e_dim, he), 0) == jnp.bitwise_and(iota((e_dim, he), 1), low)
    ).astype(F32)
    highest = lax.Precision.HIGHEST

    def make_masks():
        mkc[...] = (iota((rows, be), 0, tt) == iota((rows, be), 1, te)).astype(F32).astype(BF16)
        mks[...] = (iota((be, rows), 0, te) == iota((be, rows), 1, tt)).astype(F32).astype(BF16)
        fold[...] = (
            jnp.bitwise_and(iota((be, he), 0), low) == jnp.bitwise_and(iota((be, he), 1), low)
        ).astype(F32).astype(BF16)

    drains = []

    def gather(name, buf, recv, send, after_start, on_chip):
        own = buf.at[me]

        def push(slot, k, device):
            remote(slot, slot, send, recv.at[k], device).start()

        def arrive(slot, k):
            remote(slot, slot, send, recv.at[k], partner).wait_recv()

        def from_z(o):
            with scope(f"{name}z{o}"):
                slot = buf.at[at_z(o, yy, core)]
                arrive(slot, o)
                push(slot, nz + o, facing)
                push(slot, nc + o, partner)

        def from_y(o):
            with scope(f"{name}y{o}"):
                slot = buf.at[at_z(o, 1 - yy, core)]
                arrive(slot, nz + o)
                push(slot, nc + nz + o, partner)

        def done(o, side):
            y = 1 - yy if side else yy
            with scope(f"{name}d{side}{o}"):
                arrive(buf.at[at_z(o, y, 1 - core)], nc + nz * side + o)
            with scope(f"{name}c{side}{o}"):
                on_chip(chip_at(o, y))

        push(own, nz, facing)
        for o in near:
            push(own, o, at_z(o, yy, core))
        push(own, nc, partner)
        with scope(name + "after"):
            after_start()
        done(0, 0)
        from_z(near[0])
        from_y(0)
        for o in near[1:]:
            from_z(o)
        done(near[0], 0)
        done(0, 1)
        from_y(near[0])
        for a, b in zip(near[1:], near[:-1]):
            done(a, 0)
            from_y(a)
            done(b, 1)
        done(near[-1], 1)
        drains.append((buf.at[pl.ds(0, n - 1)], send))

    def spread(table):
        return jnp.broadcast_to(table[None], (rows // 8, 8, half)).reshape(rows, half)

    def absorb(l, j, count):
        at = pl.ds(pl.multiple_of(j * share, share), share * count)
        parts = []
        for i in range(count):
            block = xs[l, j + i].astype(F32)
            sqa[...] += block * block
            one = pl.ds(pl.multiple_of((j + i) * share, share), share)
            gain = ng_ref[l : l + 1, one].astype(F32)
            scaled = (block * gain).astype(BF16)
            nv[:, one] = scaled
            parts.append(scaled)
        both = jnp.concatenate(parts, axis=1) if count > 1 else parts[0]
        qka[...] += jnp.dot(both, wqk[l, at, :], preferred_element_type=F32)

    def clear():
        sqa[...] = jnp.zeros_like(sqa)
        qka[...] = jnp.zeros_like(qka)

    for l in range(layers):
        if l == 0:
            with scope("unpack"):
                clear()
                per = n // XPARTS
                for p in range(XPARTS):
                    loads[("x", p)].wait()
                    for j in range(p * per, (p + 1) * per):
                        piece = xr[:, :, pl.ds(j * share, share)].astype(F32)
                        xs[0, j] = piece.reshape(rows, share).astype(BF16)
            with scope("wqk"):
                loads[("q", 0)].wait()
                loads[("k", 0)].wait()
                loads["ng"].wait()
            with scope("absorb"):
                lax.fori_loop(0, n // 4, lambda i, c: (absorb(0, i * 4, 4), c)[1], 0)

        with scope(f"qk{l}"):
            scale = lax.rsqrt(jnp.sum(sqa[...], axis=1, keepdims=True) / width + EPS_RMS)
            qkg[l, me] = (qka[...] * scale).astype(BF16)
        if l == 0:
            with scope("bar"):
                pl.semaphore_wait(barrier, n - 1)

        box = {}

        def project(l=l, scale=scale, box=box):
            if l == 0:
                make_masks()
            loads[("v", l)].wait()
            loads[("g", l)].wait()
            vg = nt_dot(nv[...], wvg[l]) * scale
            box["values"] = vg[:, :he].astype(BF16)
            box["gates"] = vg[:, he:].astype(BF16).astype(F32)
            vts[...] = jnp.transpose(box["values"].astype(F32)).astype(BF16)
            loads[("s", l)].wait()
            if l == 0:
                loads["tab"].wait()
                loads["gg"].wait()
            box["mixed"] = jnp.zeros((rows, he), F32)

        def mix(h, l=l, box=box):
            qk_a = qkg[l, 2 * h].astype(F32)
            qk_b = qkg[l, 2 * h + 1].astype(F32)
            qa, ka = qk_a[:, :half], qk_a[:, half:]
            qb, kb = qk_b[:, :half], qk_b[:, half:]
            cq, sq = spread(tab_ref[0, h]), spread(tab_ref[1, h])
            ck, sk = spread(tab_ref[2, h]), spread(tab_ref[3, h])
            rq = jnp.concatenate([qa * cq - qb * sq, qb * cq + qa * sq], axis=1).astype(BF16)
            rk = jnp.concatenate([ka * ck - kb * sk, kb * ck + ka * sk], axis=1).astype(BF16)
            kh[h] = rk
            state = stv[l, :, h].reshape(be, head_dim).astype(BF16)
            scores = (nt_dot(rq, rk) * causal).astype(BF16)
            carried = nt_dot(rq, state).astype(BF16) * mkc[...]
            part = jnp.dot(scores, box["values"], preferred_element_type=F32)
            part = part + jnp.dot(carried, fold[...], preferred_element_type=F32)
            own = (iota((1, he), 1, te) == h).astype(F32)
            box["mixed"] = box["mixed"] + part * own

        gather(f"q{l}", qkg.at[l], aq_r, ag_s.at[l], project, mix)
        mixed, gates = box["mixed"], box["gates"]

        with scope(f"sums{l}"):
            sums = nt_dot(heads_of, mixed, highest)
            squares = nt_dot(heads_of, mixed * mixed, highest)
            sb[l, me] = jnp.concatenate([sums, squares], axis=1)
            for o in range(1, n):
                remote(sb.at[l, me], sb.at[l, me], st_s.at[l], st_r.at[0], lax.rem(me + o, n)).start()
            drains.append((sb.at[l, pl.ds(0, n - 1)], st_s.at[l]))

        def update(h, carry, l=l):
            at = pl.ds(pl.multiple_of(h * e_dim, e_dim), e_dim)
            tall = jnp.broadcast_to(vts[at, :][None], (seqs, e_dim, rows)).reshape(be, rows)
            fresh = jnp.dot(tall * mks[...], kh[h], preferred_element_type=F32)
            row = tab_ref[4, h][0:1, :]
            fade = jnp.concatenate([row, row], axis=1)
            state = stv[l, :, h].reshape(be, head_dim)
            stv[l, :, h] = ((state + fresh) * fade).reshape(seqs, e_dim, head_dim)
            return carry

        with scope(f"update{l}"):
            lax.fori_loop(0, heads, update, 0, unroll=True)

        with scope(f"stwait{l}"):
            others = sb.at[l, pl.ds(0, n - 1)]
            remote(others, others, st_s.at[l], st_r.at[0], partner).wait_recv()

        with scope(f"gated{l}"):
            stats = jnp.sum(sb[l], axis=0)
            mean = stats[:, :rows] / head_dim
            var = stats[:, rows:] / head_dim - mean * mean
            rstd = lax.rsqrt(var + EPS_GROUP)

            def expand(small):
                return lax.dot_general(
                    small, heads_of, (((0,), (0,)), ((), ())),
                    preferred_element_type=F32, precision=highest,
                )

            gain = jnp.dot(gg_ref[l].astype(F32), place, preferred_element_type=F32, precision=highest)
            gain = jnp.sum(gain * heads_of, axis=0, keepdims=True)
            normal = (mixed - expand(mean)) * expand(rstd) * gain
            gated = (gates / (1.0 + jnp.exp(-gates)) * normal).astype(BF16)
            loads[("o", l)].wait()

        def chunk(j, l=l, gated=gated):
            at = pl.ds(pl.multiple_of(j * share, share), share)
            return jnp.dot(gated, wo[l, :, at], preferred_element_type=F32)

        order = far + [0]
        pb_s, ys_s, rz_s = rs_s.at[l, 0], rs_s.at[l, 1], rs_s.at[l, 2]

        def offer(o, side, l=l):
            k = side * nz + o
            y = 1 - yy if side else yy
            pbs[l, k] = chunk(at_z(o, y, 1 - core)).astype(BF16)
            remote(pbs.at[l, k], pbr.at[l, k], pb_s, pb_r.at[k], partner).start()

        def paired(o, side, l=l):
            k = side * nz + o
            own = chunk(at_z(o, 1 - yy if side else yy, core))
            remote(pbs.at[l, k], pbr.at[l, k], pb_s, pb_r.at[k], partner).wait_recv()
            return own + pbr[l, k].astype(F32)

        with scope(f"rsa{l}"):
            for o in order:
                offer(o, 1)
        with scope(f"rsb{l}"):
            for o in order:
                yss[l, o] = paired(o, 1).astype(BF16)
                remote(yss.at[l, o], ysr.at[l, o], ys_s, ys_r.at[o], facing).start()
        with scope(f"rsc{l}"):
            for o in order:
                offer(o, 0)
            drains.append((pbs.at[l], pb_s))
            drains.append((yss.at[l], ys_s))
        acc = None
        for o in order:
            with scope(f"rsd{l}{o}"):
                own = paired(o, 0)
                remote(yss.at[l, o], ysr.at[l, o], ys_s, ys_r.at[o], facing).wait_recv()
                own = own + ysr[l, o].astype(F32)
                if o:
                    rss[l, o] = own.astype(BF16)
                    remote(
                        rss.at[l, o], rsr.at[l, o], rz_s, rs_r.at[o], at_z(o, yy, core)
                    ).start()
                else:
                    acc = own
        drains.append((rss.at[l, pl.ds(1, nz - 1)], rz_s))
        for o in near:
            with scope(f"rse{l}{o}"):
                remote(rss.at[l, o], rsr.at[l, o], rz_s, rs_r.at[o], facing).wait_recv()
                acc = acc + rsr[l, o].astype(F32)
        fresh_x = (xs[l, me].astype(F32) + acc).astype(BF16)
        if l + 1 < layers:
            xs[l + 1, me] = fresh_x
            loads[("q", l + 1)].wait()
            loads[("k", l + 1)].wait()
            gather(
                f"x{l}", xs.at[l + 1], ax_r, ag_s.at[layers + l], clear,
                lambda c, l=l: absorb(l + 1, 2 * c, 2),
            )
        else:
            y_ref[...] = fresh_x

    with scope("drain"):
        for ref, sem in drains:
            remote(ref, ref, sem, st_r.at[0], partner).wait_send()


def store_kernel(y_ref, state_ref, y_out, state_out, yv, sem):
    layers, seqs = state_ref.shape[:2]
    copies = []
    parts = sem.shape[0] - 1
    per = layers * seqs // parts
    for i in range(parts):
        l, s = i * per // seqs, pl.ds(i * per % seqs, per)
        copies.append(pltpu.make_async_copy(state_ref.at[l, s], state_out.at[l, s], sem.at[i]))
    for copy in copies:
        copy.start()
    yv[...] = y_ref[...].astype(F32).reshape(yv.shape).astype(BF16)
    copy = pltpu.make_async_copy(yv, y_out, sem.at[parts])
    copy.start()
    for copy in copies + [copy]:
        copy.wait()


def local(
    stream_in, state_in, norm_gain, query_weight, key_weight,
    value_weight, gate_weight, group_gain, output_weight,
):
    n = lax.axis_size("tp")
    seqs, tok, width = stream_in.shape
    layers, _, heads, e_dim, head_dim = state_in.shape
    cols = query_weight.shape[2]
    rows = seqs * tok
    he = heads * e_dim
    share = width // n
    fits = (
        cols == 128 and head_dim == 256 and he == 128 and heads == 8 and e_dim == 16
        and share % 128 == 0 and n % 4 == 0 and n & (n - 1) == 0 and rows == 128 and 8 % tok == 0
        and n == 2 * heads and seqs % 4 == 0
    )
    if not fits:
        return plain_local(
            stream_in, state_in, norm_gain, query_weight, key_weight,
            value_weight, gate_weight, group_gain, output_weight,
        )
    nc = n // 2
    be = seqs * e_dim
    hbm = pl.BlockSpec(memory_space=pltpu.HBM)
    vmem = pl.BlockSpec(memory_space=pltpu.VMEM)
    dma = pltpu.SemaphoreType.DMA
    tables = jnp.asarray(rotary_tables(heads, tok, head_dim))
    flat = lambda w: jnp.transpose(w, (0, 2, 3, 1)).reshape(layers, he, width)
    y, new_state = pl.pallas_call(
        functools.partial(kernel, n, head_dim),
        name="retention",
        out_shape=(
            pltpu.VMEM((rows, share), BF16),
            pltpu.VMEM(state_in.shape, F32),
        ),
        in_specs=[hbm] * 10,
        out_specs=(vmem, vmem),
        scratch_shapes=[
            pltpu.VMEM(norm_gain.shape, BF16),
            pltpu.VMEM(group_gain.shape, BF16),
            pltpu.VMEM(tables.shape, F32),
            pltpu.VMEM((seqs, tok, width), BF16),
            pltpu.VMEM((layers, n, rows, share), BF16),
            pltpu.VMEM((rows, width), BF16),
            pltpu.VMEM((layers, width, 2 * cols), BF16),
            pltpu.VMEM((layers, 2 * he, width), BF16),
            pltpu.VMEM((layers, he, width), BF16),
            pltpu.VMEM((layers, n, rows, 2 * cols), BF16),
            pltpu.VMEM((heads, rows, head_dim), BF16),
            pltpu.VMEM((he, rows), BF16),
            pltpu.VMEM((layers, n, heads, 2 * rows), F32),
            pltpu.VMEM((layers, nc, rows, share), BF16),
            pltpu.VMEM((layers, nc, rows, share), BF16),
            pltpu.VMEM((layers, nc // 2, rows, share), BF16),
            pltpu.VMEM((layers, nc // 2, rows, share), BF16),
            pltpu.VMEM((layers, nc // 2, rows, share), BF16),
            pltpu.VMEM((layers, nc // 2, rows, share), BF16),
            pltpu.VMEM((rows, be), BF16),
            pltpu.VMEM((be, rows), BF16),
            pltpu.VMEM((be, he), BF16),
            pltpu.VMEM((rows, share), F32),
            pltpu.VMEM((rows, 2 * cols), F32),
            dma((XPARTS + 6 * layers + 3,)),
            dma((2 * layers - 1,)),
            dma((layers,)),
            dma((layers, 3)),
            dma((n,)),
            dma((n,)),
            dma((1,)),
            dma((nc,)),
            dma((nc // 2,)),
            dma((nc // 2,)),
        ],
        compiler_params=pltpu.CompilerParams(
            collective_id=0, has_side_effects=True, vmem_limit_bytes=58500000
        ),
    )(
        stream_in, state_in, norm_gain, query_weight, key_weight,
        flat(value_weight), flat(gate_weight), group_gain,
        output_weight.reshape(layers, he, width), tables,
    )
    return pl.pallas_call(
        store_kernel,
        name="store",
        out_shape=(
            jax.ShapeDtypeStruct((seqs, tok, share), BF16),
            jax.ShapeDtypeStruct(state_in.shape, F32),
        ),
        in_specs=[vmem, vmem],
        out_specs=(hbm, hbm),
        scratch_shapes=[pltpu.VMEM((seqs, tok, share), BF16), dma((4 * layers + 1,))],
        compiler_params=pltpu.CompilerParams(vmem_limit_bytes=2 * 2**20),
    )(y, new_state)


def solution(mesh):
    in_specs = (
        P("grp", None, None),
        P(None, "grp", None, "tp", None),
        P(),
        P(None, None, "tp"),
        P(None, None, "tp"),
        P(None, None, None, "tp"),
        P(None, None, None, "tp"),
        P(None, None, "tp"),
        P(None, None, "tp", None),
    )
    out_specs = (P("grp", None, "tp"), P(None, "grp", None, "tp", None))
    return jax.shard_map(local, mesh=mesh, in_specs=in_specs, out_specs=out_specs, check_vma=False)
```

time: 92.1 us -> 82.5 us (0.90)
  Pallas kernels: 89.2 us -> 81.7 us
  local copies, waits for them, and re-layouts: 2.06 us -> 0 us
    pallas_call x1, Pallas kernels: 85.8 us -> 78.3 us  [local(): pl.pallas_call(functools.partial(kernel, n, head_dim), name='retention',...]
    reshape x2 -> x0, local copies, waits for them, and re-layouts: 2.04 us -> none  [the longest x1 1.39 us: local(): stream_in.reshape(rows, width)]
where the time goes in v1:
time: 82.5 us; the launch traced here: 82.3 us
  Pallas kernels  81.7 us (99%)
    pallas_call x1, Pallas kernels, local(): pl.pallas_call(functools.partial(kernel, n, head_dim), name='retention',...  78.3 us
    pallas_call x1, Pallas kernels, local(): pl.pallas_call(store_kernel, name='store', out_shape=(jax.ShapeDtypeStruc...  3.38 us

profile of v1, /device:TPU:0, one launch (start us, length us, event | category | flops | bytes accessed | tf_op | source)
XLA Modules:
  0.0 82.3 jit_solution(16329196457646807225)
XLA Ops:
  0.6 78.3 %retention.1 = (bf16[128,256]{1,0:T(8,128)(2,1)S(1)}, f32[2,32,8,16,256]{4,3,2,1,0:T(8,128)S(1)}) custom-call(bf16[32,4,4096]{2,1,0:T(4,128)(2,1)} %x_hbm.1, f32[2,32,8,16,256]{4,3,2,1,0:T(8,128)} %st_hbm.1, bf16[2,4096]{1,0:T(2,128)(2,1)} %ng_hbm.1, bf16[2,4096,128]{2,1,0:T(8,128)(2,1)} %qw_hbm.1, bf16[2,4096,128]{2,1,0:T(8,128)(2,1)} %kw_hbm.1, ...), custom_call_target="tpu_custom_call" | custom-call | tf_op jit(solution)/shard_map/retention/pallas_call | solution.py:565
  78.9 3.4 %store.1 = (bf16[32,4,256]{2,1,0:T(4,128)(2,1)}, f32[2,32,8,16,256]{4,3,2,1,0:T(8,128)}) custom-call(bf16[128,256]{1,0:T(8,128)(2,1)S(1)} %get-tuple-element.4.y_ref, f32[2,32,8,16,256]{4,3,2,1,0:T(8,128)S(1)} %get-tuple-element.5.state_ref), custom_call_target="tpu_custom_call" | custom-call | tf_op jit(solution)/shard_map/store/pallas_call | solution.py:618

commit v2 on v1

--- a/solution.py
+++ b/solution.py
@@ -174,8 +174,8 @@
     n, head_dim,
     x_hbm, st_hbm, ng_hbm, qw_hbm, kw_hbm, vw_hbm, gw_hbm, gg_hbm, ow_hbm, tab_hbm,
     y_ref, stv,
-    ng_ref, gg_ref, tab_ref, xr, xs, nv, wqk, wvg, wo, qkg, kh, vts, sb, pbs, pbr, yss, ysr, rss, rsr, mkc, mks, fold, sqa, qka,
-    lsem, ag_s, st_s, rs_s, aq_r, ax_r, st_r, pb_r, ys_r, rs_r,
+    ng_ref, gg_ref, tab_ref, xr, xs, nv, wqk, wvg, wo, qg, kg, sc, vts, sb, pbs, pbr, yss, ysr, rss, rsr, mkc, mks, fold, sqa, qka,
+    lsem, ag_s, st_s, rs_s, aq_r, ak_r, ax_r, sc_r, st_r, pb_r, ys_r, rs_r,
 ):
     layers, seqs, heads, e_dim, _ = st_hbm.shape
     tok = x_hbm.shape[1]
@@ -239,8 +239,11 @@
         )
 
     for l in range(layers):
-        load(("q", l), qw_hbm.at[l], wqk.at[l, :, pl.ds(0, cols)])
-        load(("k", l), kw_hbm.at[l], wqk.at[l, :, pl.ds(cols, cols)])
+        deep = wide if l == 0 else width
+        for j in range(width // deep):
+            at = pl.ds(j * deep, deep)
+            load(("q", l, j), qw_hbm.at[l, at], wqk.at[l, at, pl.ds(0, cols)])
+            load(("k", l, j), kw_hbm.at[l, at], wqk.at[l, at, pl.ds(cols, cols)])
         load(("v", l), vw_hbm.at[l], wvg.at[l, pl.ds(0, he)])
         load(("g", l), gw_hbm.at[l], wvg.at[l, pl.ds(he, he)])
         load(("s", l), st_hbm.at[l], stv.at[l])
@@ -264,6 +267,10 @@
     place = (
         iota((e_dim, he), 0) == jnp.bitwise_and(iota((e_dim, he), 1), low)
     ).astype(F32)
+    same = (iota((rows, rows), 0, tt) == iota((rows, rows), 1, tt)).astype(F32)
+    pick = (
+        jnp.bitwise_and(iota((8, rows), 1), tok - 1) == iota((8, rows), 0)
+    ).astype(F32).astype(BF16)
     highest = lax.Precision.HIGHEST
 
     def make_masks():
@@ -275,64 +282,82 @@
 
     drains = []
 
-    def gather(name, buf, recv, send, after_start, on_chip):
-        own = buf.at[me]
-
+    def ring(name, buf, recv, send):
         def push(slot, k, device):
             remote(slot, slot, send, recv.at[k], device).start()
 
         def arrive(slot, k):
             remote(slot, slot, send, recv.at[k], partner).wait_recv()
+
+        def start(others=True, other_core=True):
+            own = buf.at[me]
+            if other_core:
+                push(own, nc, partner)
+            if others:
+                push(own, nz, facing)
+                for o in near:
+                    push(own, o, at_z(o, yy, core))
+                drains.append((buf.at[pl.ds(0, n - 1)], send))
+
+        def last(k):
+            return k if recv.shape[0] == n else nc if k == nc else nc + 1
 
         def from_z(o):
             with scope(f"{name}z{o}"):
                 slot = buf.at[at_z(o, yy, core)]
                 arrive(slot, o)
                 push(slot, nz + o, facing)
-                push(slot, nc + o, partner)
+                push(slot, last(nc + o), partner)
 
         def from_y(o):
             with scope(f"{name}y{o}"):
                 slot = buf.at[at_z(o, 1 - yy, core)]
                 arrive(slot, nz + o)
-                push(slot, nc + nz + o, partner)
+                push(slot, last(nc + nz + o), partner)
 
         def done(o, side):
-            y = 1 - yy if side else yy
             with scope(f"{name}d{side}{o}"):
-                arrive(buf.at[at_z(o, y, 1 - core)], nc + nz * side + o)
+                arrive(buf.at[at_z(o, 1 - yy if side else yy, 1 - core)], nc + nz * side + o)
+
+        def done_rest():
+            with scope(name + "rest"):
+                arrive(buf.at[pl.ds(0, nc - 1)], nc + 1)
+
+        return start, from_z, from_y, done, done_rest
+
+    def in_order(name, from_z, from_y, done, on_chip):
+        def use(o, side):
+            done(o, side)
             with scope(f"{name}c{side}{o}"):
-                on_chip(chip_at(o, y))
-
-        push(own, nz, facing)
-        for o in near:
-            push(own, o, at_z(o, yy, core))
-        push(own, nc, partner)
-        with scope(name + "after"):
-            after_start()
-        done(0, 0)
+                on_chip(o, side)
+
+        use(0, 0)
         from_z(near[0])
         from_y(0)
         for o in near[1:]:
             from_z(o)
-        done(near[0], 0)
-        done(0, 1)
+        use(near[0], 0)
+        use(0, 1)
         from_y(near[0])
         for a, b in zip(near[1:], near[:-1]):
-            done(a, 0)
+            use(a, 0)
             from_y(a)
-            done(b, 1)
-        done(near[-1], 1)
-        drains.append((buf.at[pl.ds(0, n - 1)], send))
+            use(b, 1)
+        use(near[-1], 1)
 
     def spread(table):
         return jnp.broadcast_to(table[None], (rows // 8, 8, half)).reshape(rows, half)
 
-    def absorb(l, j, count):
+    def rotated(buf, l, h, table):
+        a, b = buf[l, 2 * h].astype(F32), buf[l, 2 * h + 1].astype(F32)
+        cosine, sine = spread(tab_ref[table, h]), spread(tab_ref[table + 1, h])
+        return jnp.concatenate([a * cosine - b * sine, b * cosine + a * sine], axis=1).astype(BF16)
+
+    def absorb(l, j, count, block_of):
         at = pl.ds(pl.multiple_of(j * share, share), share * count)
         parts = []
         for i in range(count):
-            block = xs[l, j + i].astype(F32)
+            block = block_of(j + i)
             sqa[...] += block * block
             one = pl.ds(pl.multiple_of((j + i) * share, share), share)
             gain = ng_ref[l : l + 1, one].astype(F32)
@@ -342,71 +367,87 @@
         both = jnp.concatenate(parts, axis=1) if count > 1 else parts[0]
         qka[...] += jnp.dot(both, wqk[l, at, :], preferred_element_type=F32)
 
+    def unpack(j):
+        block = xr[:, :, pl.ds(j * share, share)].astype(F32).reshape(rows, share)
+        xs[0, j] = block.astype(BF16)
+        return block
+
     def clear():
         sqa[...] = jnp.zeros_like(sqa)
         qka[...] = jnp.zeros_like(qka)
 
     for l in range(layers):
         if l == 0:
-            with scope("unpack"):
+            with scope("absorb"):
                 clear()
                 per = n // XPARTS
+                loads["ng"].wait()
                 for p in range(XPARTS):
-                    loads[("x", p)].wait()
-                    for j in range(p * per, (p + 1) * per):
-                        piece = xr[:, :, pl.ds(j * share, share)].astype(F32)
-                        xs[0, j] = piece.reshape(rows, share).astype(BF16)
-            with scope("wqk"):
-                loads[("q", 0)].wait()
-                loads[("k", 0)].wait()
-                loads["ng"].wait()
-            with scope("absorb"):
-                lax.fori_loop(0, n // 4, lambda i, c: (absorb(0, i * 4, 4), c)[1], 0)
+                    for name in (("x", p), ("q", 0, p), ("k", 0, p)):
+                        loads[name].wait()
+                    absorb(0, p * per, per, unpack)
 
         with scope(f"qk{l}"):
             scale = lax.rsqrt(jnp.sum(sqa[...], axis=1, keepdims=True) / width + EPS_RMS)
-            qkg[l, me] = (qka[...] * scale).astype(BF16)
+            both = (qka[...] * scale).astype(BF16)
+            qg[l, me] = both[:, :cols]
+            kg[l, me] = both[:, cols:]
         if l == 0:
             with scope("bar"):
                 pl.semaphore_wait(barrier, n - 1)
 
-        box = {}
-
-        def project(l=l, scale=scale, box=box):
-            if l == 0:
+        q_start, q_z, q_y, q_done, _ = ring(f"q{l}", qg.at[l], aq_r, ag_s.at[l, 0])
+        k_start, k_z, k_y, k_done, k_rest = ring(f"k{l}", kg.at[l], ak_r, ag_s.at[l, 1])
+        q_start()
+        k_start(others=False)
+        if l == 0:
+            with scope("masks"):
                 make_masks()
+                loads["tab"].wait()
+                loads["gg"].wait()
+        q_done(0, 0)
+        k_done(0, 0)
+        with scope(f"scores{l}"):
+            rk = rotated(kg, l, chip, 2)
+            scores = (nt_dot(rotated(qg, l, chip, 0), rk) * causal).astype(BF16)
+            sc[l, chip] = nt_dot(pick, scores)
+            for o, side in [(o, 0) for o in near] + [(0, 1)] + [(o, 1) for o in near]:
+                slot = sc.at[l, chip]
+                remote(
+                    slot, slot, ag_s.at[l, 2], sc_r.at[side * nz + o],
+                    at_z(o, 1 - yy if side else yy, core),
+                ).start()
+            drains.append((sc.at[l, pl.ds(0, nc - 1)], ag_s.at[l, 2]))
+        k_start(other_core=False)
+
+        with scope(f"vg{l}"):
             loads[("v", l)].wait()
             loads[("g", l)].wait()
             vg = nt_dot(nv[...], wvg[l]) * scale
-            box["values"] = vg[:, :he].astype(BF16)
-            box["gates"] = vg[:, he:].astype(BF16).astype(F32)
-            vts[...] = jnp.transpose(box["values"].astype(F32)).astype(BF16)
+            values = vg[:, :he].astype(BF16)
+            gates = vg[:, he:].astype(BF16).astype(F32)
+            vts[...] = jnp.transpose(values.astype(F32)).astype(BF16)
             loads[("s", l)].wait()
-            if l == 0:
-                loads["tab"].wait()
-                loads["gg"].wait()
-            box["mixed"] = jnp.zeros((rows, he), F32)
-
-        def mix(h, l=l, box=box):
-            qk_a = qkg[l, 2 * h].astype(F32)
-            qk_b = qkg[l, 2 * h + 1].astype(F32)
-            qa, ka = qk_a[:, :half], qk_a[:, half:]
-            qb, kb = qk_b[:, :half], qk_b[:, half:]
-            cq, sq = spread(tab_ref[0, h]), spread(tab_ref[1, h])
-            ck, sk = spread(tab_ref[2, h]), spread(tab_ref[3, h])
-            rq = jnp.concatenate([qa * cq - qb * sq, qb * cq + qa * sq], axis=1).astype(BF16)
-            rk = jnp.concatenate([ka * ck - kb * sk, kb * ck + ka * sk], axis=1).astype(BF16)
-            kh[h] = rk
+        box = {"mixed": jnp.zeros((rows, he), F32)}
+
+        def mix(o, side, l=l, box=box, values=values):
+            h = chip_at(o, 1 - yy if side else yy)
+            rq = rotated(qg, l, h, 0)
             state = stv[l, :, h].reshape(be, head_dim).astype(BF16)
-            scores = (nt_dot(rq, rk) * causal).astype(BF16)
             carried = nt_dot(rq, state).astype(BF16) * mkc[...]
-            part = jnp.dot(scores, box["values"], preferred_element_type=F32)
-            part = part + jnp.dot(carried, fold[...], preferred_element_type=F32)
+            part = jnp.dot(carried, fold[...], preferred_element_type=F32)
+            if o or side:
+                slot = sc.at[l, h]
+                remote(slot, slot, ag_s.at[l, 2], sc_r.at[side * nz + o], partner).wait_recv()
+            full = lax.dot_general(
+                sc[l, h].astype(BF16), pick, (((0,), (0,)), ((), ())), preferred_element_type=F32
+            )
+            part = part + jnp.dot((full * same).astype(BF16), values, preferred_element_type=F32)
             own = (iota((1, he), 1, te) == h).astype(F32)
             box["mixed"] = box["mixed"] + part * own
 
-        gather(f"q{l}", qkg.at[l], aq_r, ag_s.at[l], project, mix)
-        mixed, gates = box["mixed"], box["gates"]
+        in_order(f"q{l}", q_z, q_y, lambda o, s: None if o == s == 0 else q_done(o, s), mix)
+        mixed = box["mixed"]
 
         with scope(f"sums{l}"):
             sums = nt_dot(heads_of, mixed, highest)
@@ -416,18 +457,19 @@
                 remote(sb.at[l, me], sb.at[l, me], st_s.at[l], st_r.at[0], lax.rem(me + o, n)).start()
             drains.append((sb.at[l, pl.ds(0, n - 1)], st_s.at[l]))
 
+        for o in near:
+            k_z(o)
+        k_y(0)
+
         def update(h, carry, l=l):
             at = pl.ds(pl.multiple_of(h * e_dim, e_dim), e_dim)
             tall = jnp.broadcast_to(vts[at, :][None], (seqs, e_dim, rows)).reshape(be, rows)
-            fresh = jnp.dot(tall * mks[...], kh[h], preferred_element_type=F32)
+            fresh = jnp.dot(tall * mks[...], rotated(kg, l, h, 2), preferred_element_type=F32)
             row = tab_ref[4, h][0:1, :]
             fade = jnp.concatenate([row, row], axis=1)
             state = stv[l, :, h].reshape(be, head_dim)
             stv[l, :, h] = ((state + fresh) * fade).reshape(seqs, e_dim, head_dim)
             return carry
-
-        with scope(f"update{l}"):
-            lax.fori_loop(0, heads, update, 0, unroll=True)
 
         with scope(f"stwait{l}"):
             others = sb.at[l, pl.ds(0, n - 1)]
@@ -482,6 +524,11 @@
                 offer(o, 0)
             drains.append((pbs.at[l], pb_s))
             drains.append((yss.at[l], ys_s))
+        for o in near:
+            k_y(o)
+        k_rest()
+        with scope(f"update{l}"):
+            lax.fori_loop(0, heads, update, 0, unroll=True)
         acc = None
         for o in order:
             with scope(f"rsd{l}{o}"):
@@ -503,12 +550,17 @@
         fresh_x = (xs[l, me].astype(F32) + acc).astype(BF16)
         if l + 1 < layers:
             xs[l + 1, me] = fresh_x
-            loads[("q", l + 1)].wait()
-            loads[("k", l + 1)].wait()
-            gather(
-                f"x{l}", xs.at[l + 1], ax_r, ag_s.at[layers + l], clear,
-                lambda c, l=l: absorb(l + 1, 2 * c, 2),
-            )
+            loads[("q", l + 1, 0)].wait()
+            loads[("k", l + 1, 0)].wait()
+            x_start, x_z, x_y, x_done, _ = ring(f"x{l}", xs.at[l + 1], ax_r, ag_s.at[l, 3])
+            x_start()
+            clear()
+
+            def take(o, side, l=l):
+                c = chip_at(o, 1 - yy if side else yy)
+                absorb(l + 1, 2 * c, 2, lambda j: xs[l + 1, j].astype(F32))
+
+            in_order(f"x{l}", x_z, x_y, x_done, take)
         else:
             y_ref[...] = fresh_x
 
@@ -581,8 +633,9 @@
             pltpu.VMEM((layers, width, 2 * cols), BF16),
             pltpu.VMEM((layers, 2 * he, width), BF16),
             pltpu.VMEM((layers, he, width), BF16),
-            pltpu.VMEM((layers, n, rows, 2 * cols), BF16),
-            pltpu.VMEM((heads, rows, head_dim), BF16),
+            pltpu.VMEM((layers, n, rows, cols), BF16),
+            pltpu.VMEM((layers, n, rows, cols), BF16),
+            pltpu.VMEM((layers, heads, 8, rows), F32),
             pltpu.VMEM((he, rows), BF16),
             pltpu.VMEM((layers, n, heads, 2 * rows), F32),
             pltpu.VMEM((layers, nc, rows, share), BF16),
@@ -596,12 +649,14 @@
             pltpu.VMEM((be, he), BF16),
             pltpu.VMEM((rows, share), F32),
             pltpu.VMEM((rows, 2 * cols), F32),
-            dma((XPARTS + 6 * layers + 3,)),
-            dma((2 * layers - 1,)),
+            dma((3 * XPARTS + 6 * layers + 1,)),
+            dma((layers, 4)),
             dma((layers,)),
             dma((layers, 3)),
             dma((n,)),
+            dma((nc + 2,)),
             dma((n,)),
+            dma((nc,)),
             dma((1,)),
             dma((nc,)),
             dma((nc // 2,)),

time: 82.5 us -> 80.3 us (0.973)
  Pallas kernels: 81.7 us -> 79.5 us
    pallas_call x1, Pallas kernels: 78.3 us -> 76.1 us  [local(): pl.pallas_call(functools.partial(kernel, n, head_dim), name='retention',...]
where the time goes in v2:
time: 80.3 us; the launch traced here: 80.1 us
  Pallas kernels  79.5 us (99%)
    pallas_call x1, Pallas kernels, local(): pl.pallas_call(functools.partial(kernel, n, head_dim), name='retention',...  76.1 us
    pallas_call x1, Pallas kernels, local(): pl.pallas_call(store_kernel, name='store', out_shape=(jax.ShapeDtypeStruc...  3.38 us

profile of v2, /device:TPU:0, one launch (start us, length us, event | category | flops | bytes accessed | tf_op | source)
XLA Modules:
  0.0 80.1 jit_solution(2447325522540511684)
XLA Ops:
  0.6 76.1 %retention.1 = (bf16[128,256]{1,0:T(8,128)(2,1)S(1)}, f32[2,32,8,16,256]{4,3,2,1,0:T(8,128)S(1)}) custom-call(bf16[32,4,4096]{2,1,0:T(4,128)(2,1)} %x_hbm.1, f32[2,32,8,16,256]{4,3,2,1,0:T(8,128)} %st_hbm.1, bf16[2,4096]{1,0:T(2,128)(2,1)} %ng_hbm.1, bf16[2,4096,128]{2,1,0:T(8,128)(2,1)} %qw_hbm.1, bf16[2,4096,128]{2,1,0:T(8,128)(2,1)} %kw_hbm.1, ...), custom_call_target="tpu_custom_call" | custom-call | tf_op jit(solution)/shard_map/retention/pallas_call | solution.py:617
  76.7 3.4 %store.1 = (bf16[32,4,256]{2,1,0:T(4,128)(2,1)}, f32[2,32,8,16,256]{4,3,2,1,0:T(8,128)}) custom-call(bf16[128,256]{1,0:T(8,128)(2,1)S(1)} %get-tuple-element.4.y_ref, f32[2,32,8,16,256]{4,3,2,1,0:T(8,128)S(1)} %get-tuple-element.5.state_ref), custom_call_target="tpu_custom_call" | custom-call | tf_op jit(solution)/shard_map/store/pallas_call | solution.py:673

commit v3 on v2

--- a/solution.py
+++ b/solution.py
@@ -174,7 +174,7 @@
     n, head_dim,
     x_hbm, st_hbm, ng_hbm, qw_hbm, kw_hbm, vw_hbm, gw_hbm, gg_hbm, ow_hbm, tab_hbm,
     y_ref, stv,
-    ng_ref, gg_ref, tab_ref, xr, xs, nv, wqk, wvg, wo, qg, kg, sc, vts, sb, pbs, pbr, yss, ysr, rss, rsr, mkc, mks, fold, sqa, qka,
+    ng_ref, gg_ref, tab_ref, xr, xs, nv, wqk, wvg, wo, qg, kg, sc, vts, vb, sb, pbs, pbr, yss, ysr, rss, rsr, mkc, mks, fold, sqa, qka, osum,
     lsem, ag_s, st_s, rs_s, aq_r, ak_r, ax_r, sc_r, st_r, pb_r, ys_r, rs_r,
 ):
     layers, seqs, heads, e_dim, _ = st_hbm.shape
@@ -267,7 +267,15 @@
     place = (
         iota((e_dim, he), 0) == jnp.bitwise_and(iota((e_dim, he), 1), low)
     ).astype(F32)
-    same = (iota((rows, rows), 0, tt) == iota((rows, rows), 1, tt)).astype(F32)
+    nth = jnp.concatenate(
+        [
+            (
+                jnp.left_shift(iota((rows, rows), 0, tt), tt) + t == iota((rows, rows), 1)
+            ).astype(F32).astype(BF16)
+            for t in range(tok)
+        ],
+        axis=0,
+    )
     pick = (
         jnp.bitwise_and(iota((8, rows), 1), tok - 1) == iota((8, rows), 0)
     ).astype(F32).astype(BF16)
@@ -281,8 +289,12 @@
         ).astype(F32).astype(BF16)
 
     drains = []
-
-    def ring(name, buf, recv, send):
+    halves = [pl.ds(i * (rows // 2), rows // 2) for i in range(2)]
+
+    def ring(name, buf, recv, send, at=None):
+        def slot_of(j):
+            return buf.at[j] if at is None else buf.at[j, at]
+
         def push(slot, k, device):
             remote(slot, slot, send, recv.at[k], device).start()
 
@@ -290,60 +302,62 @@
             remote(slot, slot, send, recv.at[k], partner).wait_recv()
 
         def start(others=True, other_core=True):
-            own = buf.at[me]
+            own = slot_of(me)
             if other_core:
                 push(own, nc, partner)
             if others:
                 push(own, nz, facing)
                 for o in near:
                     push(own, o, at_z(o, yy, core))
-                drains.append((buf.at[pl.ds(0, n - 1)], send))
+                drains.append((slot_of(pl.ds(0, n - 1)), send))
 
         def last(k):
             return k if recv.shape[0] == n else nc if k == nc else nc + 1
 
         def from_z(o):
             with scope(f"{name}z{o}"):
-                slot = buf.at[at_z(o, yy, core)]
+                slot = slot_of(at_z(o, yy, core))
                 arrive(slot, o)
                 push(slot, nz + o, facing)
                 push(slot, last(nc + o), partner)
 
         def from_y(o):
             with scope(f"{name}y{o}"):
-                slot = buf.at[at_z(o, 1 - yy, core)]
+                slot = slot_of(at_z(o, 1 - yy, core))
                 arrive(slot, nz + o)
                 push(slot, last(nc + nz + o), partner)
 
         def done(o, side):
             with scope(f"{name}d{side}{o}"):
-                arrive(buf.at[at_z(o, 1 - yy if side else yy, 1 - core)], nc + nz * side + o)
+                arrive(slot_of(at_z(o, 1 - yy if side else yy, 1 - core)), nc + nz * side + o)
 
         def done_rest():
             with scope(name + "rest"):
-                arrive(buf.at[pl.ds(0, nc - 1)], nc + 1)
+                arrive(slot_of(pl.ds(0, nc - 1)), nc + 1)
 
         return start, from_z, from_y, done, done_rest
 
-    def in_order(name, from_z, from_y, done, on_chip):
-        def use(o, side):
-            done(o, side)
-            with scope(f"{name}c{side}{o}"):
-                on_chip(o, side)
-
-        use(0, 0)
+    def in_order(name, from_z, from_y, done, on_chip, between=lambda: None):
+        def use(*which):
+            for o, side in which:
+                done(o, side)
+            with scope(f"{name}c{which[0][1]}{which[0][0]}"):
+                on_chip(which)
+
+        use((0, 0))
         from_z(near[0])
         from_y(0)
         for o in near[1:]:
             from_z(o)
-        use(near[0], 0)
-        use(0, 1)
+        use((near[0], 0), (0, 1))
         from_y(near[0])
-        for a, b in zip(near[1:], near[:-1]):
-            use(a, 0)
-            from_y(a)
-            use(b, 1)
-        use(near[-1], 1)
+        use(*[(o, 0) for o in near[1:]])
+        for o in near[1:-1]:
+            from_y(o)
+        between()
+        from_y(near[-1])
+        use(*[(o, 1) for o in near[:-1]])
+        use((near[-1], 1))
 
     def spread(table):
         return jnp.broadcast_to(table[None], (rows // 8, 8, half)).reshape(rows, half)
@@ -411,10 +425,10 @@
             rk = rotated(kg, l, chip, 2)
             scores = (nt_dot(rotated(qg, l, chip, 0), rk) * causal).astype(BF16)
             sc[l, chip] = nt_dot(pick, scores)
-            for o, side in [(o, 0) for o in near] + [(0, 1)] + [(o, 1) for o in near]:
+            for o, side in [(o, side) for o in far for side in (1, 0)] + [(0, 1)]:
                 slot = sc.at[l, chip]
                 remote(
-                    slot, slot, ag_s.at[l, 2], sc_r.at[side * nz + o],
+                    slot, slot, ag_s.at[l, 2], sc_r.at[0],
                     at_z(o, 1 - yy if side else yy, core),
                 ).start()
             drains.append((sc.at[l, pl.ds(0, nc - 1)], ag_s.at[l, 2]))
@@ -427,34 +441,42 @@
             values = vg[:, :he].astype(BF16)
             gates = vg[:, he:].astype(BF16).astype(F32)
             vts[...] = jnp.transpose(values.astype(F32)).astype(BF16)
+            vb[...] = jnp.dot(nth, values, preferred_element_type=F32).reshape(tok, rows, he)
             loads[("s", l)].wait()
         box = {"mixed": jnp.zeros((rows, he), F32)}
 
-        def mix(o, side, l=l, box=box, values=values):
+        def carry_one(o, side, l=l):
             h = chip_at(o, 1 - yy if side else yy)
             rq = rotated(qg, l, h, 0)
             state = stv[l, :, h].reshape(be, head_dim).astype(BF16)
             carried = nt_dot(rq, state).astype(BF16) * mkc[...]
             part = jnp.dot(carried, fold[...], preferred_element_type=F32)
-            if o or side:
-                slot = sc.at[l, h]
-                remote(slot, slot, ag_s.at[l, 2], sc_r.at[side * nz + o], partner).wait_recv()
-            full = lax.dot_general(
-                sc[l, h].astype(BF16), pick, (((0,), (0,)), ((), ())), preferred_element_type=F32
-            )
-            part = part + jnp.dot((full * same).astype(BF16), values, preferred_element_type=F32)
-            own = (iota((1, he), 1, te) == h).astype(F32)
-            box["mixed"] = box["mixed"] + part * own
-
-        in_order(f"q{l}", q_z, q_y, lambda o, s: None if o == s == 0 else q_done(o, s), mix)
+            return part * (iota((1, he), 1, te) == h).astype(F32)
+
+        def intra(l=l, box=box):
+            with scope(f"intra{l}"):
+                others = sc.at[l, pl.ds(0, nc - 1)]
+                remote(others, others, ag_s.at[l, 2], sc_r.at[0], partner).wait_recv()
+                flat = jnp.concatenate([sc[l, :, t, :] for t in range(tok)], axis=1).astype(BF16)
+                wide = lax.dot_general(
+                    flat, heads_of.astype(BF16), (((0,), (0,)), ((), ())), preferred_element_type=F32
+                )
+                box["mixed"] = box["mixed"] + jnp.sum(wide.reshape(tok, rows, he) * vb[...], axis=0)
+
+        def mix(which, box=box):
+            for o, side in which:
+                box["mixed"] = box["mixed"] + carry_one(o, side)
+
+        in_order(f"q{l}", q_z, q_y, lambda o, s: None if o == s == 0 else q_done(o, s), mix, intra)
         mixed = box["mixed"]
 
         with scope(f"sums{l}"):
             sums = nt_dot(heads_of, mixed, highest)
             squares = nt_dot(heads_of, mixed * mixed, highest)
             sb[l, me] = jnp.concatenate([sums, squares], axis=1)
-            for o in range(1, n):
-                remote(sb.at[l, me], sb.at[l, me], st_s.at[l], st_r.at[0], lax.rem(me + o, n)).start()
+            peers = [at_z(o, y, c) for o in far for y in (1 - yy, yy) for c in (core, 1 - core)]
+            for device in peers + [at_z(0, 1 - yy, 1 - core), facing, partner]:
+                remote(sb.at[l, me], sb.at[l, me], st_s.at[l], st_r.at[0], device).start()
             drains.append((sb.at[l, pl.ds(0, n - 1)], st_s.at[l]))
 
         for o in near:
@@ -471,6 +493,11 @@
             stv[l, :, h] = ((state + fresh) * fade).reshape(seqs, e_dim, head_dim)
             return carry
 
+        with scope(f"silu{l}"):
+            gain = jnp.dot(gg_ref[l].astype(F32), place, preferred_element_type=F32, precision=highest)
+            gain = jnp.sum(gain * heads_of, axis=0, keepdims=True)
+            gains = gates / (1.0 + jnp.exp(-gates)) * gain
+
         with scope(f"stwait{l}"):
             others = sb.at[l, pl.ds(0, n - 1)]
             remote(others, others, st_s.at[l], st_r.at[0], partner).wait_recv()
@@ -487,10 +514,7 @@
                     preferred_element_type=F32, precision=highest,
                 )
 
-            gain = jnp.dot(gg_ref[l].astype(F32), place, preferred_element_type=F32, precision=highest)
-            gain = jnp.sum(gain * heads_of, axis=0, keepdims=True)
-            normal = (mixed - expand(mean)) * expand(rstd) * gain
-            gated = (gates / (1.0 + jnp.exp(-gates)) * normal).astype(BF16)
+            gated = ((mixed - expand(mean)) * expand(rstd) * gains).astype(BF16)
             loads[("o", l)].wait()
 
         def chunk(j, l=l, gated=gated):
@@ -512,57 +536,133 @@
             remote(pbs.at[l, k], pbr.at[l, k], pb_s, pb_r.at[k], partner).wait_recv()
             return own + pbr[l, k].astype(F32)
 
+        early = order[0]
+        later = order[1:]
+        tail = halves[1]
+
+        def hop(o, at, l=l):
+            src, dst = yss.at[l, o, at], ysr.at[l, o, at]
+            return remote(src, dst, ys_s, ys_r.at[halves.index(at), o], facing)
+
+        def turn(o, at, l=l):
+            src, dst = rss.at[l, o, at], rsr.at[l, o, at]
+            return remote(src, dst, rz_s, rs_r.at[halves.index(at), o], at_z(o, yy, core))
+
+        def cross(l=l):
+            return remote(rss.at[l, 0, tail], rsr.at[l, 0, tail], rz_s, rs_r.at[1, 0], at_z(early, yy, core))
+
         with scope(f"rsa{l}"):
-            for o in order:
+            offer(early, 1)
+            offer(early, 0)
+            for o in later:
                 offer(o, 1)
         with scope(f"rsb{l}"):
-            for o in order:
+            both = paired(early, 1).astype(BF16)
+            yss[l, early] = both
+            hop(early, halves[0]).start()
+            rss[l, 0, tail] = both[rows // 2 :]
+            cross().start()
+            osum[early] = paired(early, 0)
+            rss[l, early, tail] = osum[early, tail].astype(BF16)
+            turn(early, tail).start()
+            for o in later[:-1]:
                 yss[l, o] = paired(o, 1).astype(BF16)
-                remote(yss.at[l, o], ysr.at[l, o], ys_s, ys_r.at[o], facing).start()
+                hop(o, halves[0]).start()
+            osum[nz] = paired(0, 1)
+            yss[l, 0, halves[0]] = osum[nz, halves[0]].astype(BF16)
+            hop(0, halves[0]).start()
+            for o in later[:-1]:
+                hop(o, tail).start()
         with scope(f"rsc{l}"):
-            for o in order:
+            for o in later:
                 offer(o, 0)
+            for o in near:
+                k_y(o)
             drains.append((pbs.at[l], pb_s))
-            drains.append((yss.at[l], ys_s))
-        for o in near:
-            k_y(o)
+            drains.append((pbs.at[l, pl.ds(0, 2 * nz - 1), tail], ys_s))
+            drains.append((pbs.at[l, pl.ds(0, 2 * nz - 1), tail], rz_s))
+        with scope(f"own{l}"):
+            for o in later:
+                osum[o] = paired(o, 0)
+
+        def join(o, at, l=l):
+            with scope(f"rsd{l}{o}"):
+                hop(o, at).wait_recv()
+                own = osum[o, at] + ysr[l, o, at].astype(F32)
+                if o:
+                    rss[l, o, at] = own.astype(BF16)
+                    turn(o, at).start()
+                else:
+                    osum[o, at] = own
+
+        def finish(at, l=l):
+            acc = osum[0, at] + xs[l, me, at].astype(F32)
+            with scope(f"rse{l}"):
+                for o in near:
+                    turn(o, at).wait_recv()
+                    acc = acc + rsr[l, o, at].astype(F32)
+            return acc.astype(BF16)
+
+        for o in order:
+            join(o, halves[0])
+        for o in later[:-1]:
+            join(o, tail)
+        with scope(f"cross{l}"):
+            cross().wait_recv()
+            yss[l, 0, tail] = (osum[nz, tail] + rsr[l, 0, tail].astype(F32)).astype(BF16)
+            hop(0, tail).start()
         k_rest()
         with scope(f"update{l}"):
             lax.fori_loop(0, heads, update, 0, unroll=True)
-        acc = None
-        for o in order:
-            with scope(f"rsd{l}{o}"):
-                own = paired(o, 0)
-                remote(yss.at[l, o], ysr.at[l, o], ys_s, ys_r.at[o], facing).wait_recv()
-                own = own + ysr[l, o].astype(F32)
-                if o:
-                    rss[l, o] = own.astype(BF16)
-                    remote(
-                        rss.at[l, o], rsr.at[l, o], rz_s, rs_r.at[o], at_z(o, yy, core)
-                    ).start()
-                else:
-                    acc = own
-        drains.append((rss.at[l, pl.ds(1, nz - 1)], rz_s))
-        for o in near:
-            with scope(f"rse{l}{o}"):
-                remote(rss.at[l, o], rsr.at[l, o], rz_s, rs_r.at[o], facing).wait_recv()
-                acc = acc + rsr[l, o].astype(F32)
-        fresh_x = (xs[l, me].astype(F32) + acc).astype(BF16)
-        if l + 1 < layers:
-            xs[l + 1, me] = fresh_x
-            loads[("q", l + 1, 0)].wait()
-            loads[("k", l + 1, 0)].wait()
-            x_start, x_z, x_y, x_done, _ = ring(f"x{l}", xs.at[l + 1], ax_r, ag_s.at[l, 3])
-            x_start()
-            clear()
-
-            def take(o, side, l=l):
-                c = chip_at(o, 1 - yy if side else yy)
-                absorb(l + 1, 2 * c, 2, lambda j: xs[l + 1, j].astype(F32))
-
-            in_order(f"x{l}", x_z, x_y, x_done, take)
-        else:
-            y_ref[...] = fresh_x
+        if l + 1 == layers:
+            y_ref[halves[0], :] = finish(halves[0])
+            join(0, tail)
+            y_ref[tail, :] = finish(tail)
+            continue
+
+        rings = []
+        clear()
+        for i, at in enumerate(halves):
+            rings.append(ring(f"x{l}{i}", xs.at[l + 1], ax_r.at[i], ag_s.at[l, 3 + i], at))
+            if i:
+                join(0, tail)
+            xs[l + 1, me, at] = finish(at)
+            rings[i][0]()
+        loads[("q", l + 1, 0)].wait()
+        loads[("k", l + 1, 0)].wait()
+        (_, az, ay, ad, _), (_, bz, by, bd, _) = rings
+
+        def use(*which, l=l):
+            for o, side in which:
+                ad(o, side)
+                bd(o, side)
+            with scope(f"x{l}c{which[0][1]}{which[0][0]}"):
+                for o, side in which:
+                    c = chip_at(o, 1 - yy if side else yy)
+                    absorb(l + 1, 2 * c, 2, lambda j: xs[l + 1, j].astype(F32))
+
+        first, rest, end = near[0], near[1:], near[-1]
+        az(first)
+        ay(0)
+        for o in rest:
+            az(o)
+        bz(first)
+        ay(first)
+        by(0)
+        use((0, 0))
+        for o in rest[:-1]:
+            ay(o)
+            bz(o)
+        ay(end)
+        bz(end)
+        use((first, 0), (0, 1))
+        by(first)
+        use(*[(o, 0) for o in rest])
+        for o in rest[:-1]:
+            by(o)
+        by(end)
+        use(*[(o, 1) for o in near[:-1]])
+        use((end, 1))
 
     with scope("drain"):
         for ref, sem in drains:
@@ -637,6 +737,7 @@
             pltpu.VMEM((layers, n, rows, cols), BF16),
             pltpu.VMEM((layers, heads, 8, rows), F32),
             pltpu.VMEM((he, rows), BF16),
+            pltpu.VMEM((tok, rows, he), F32),
             pltpu.VMEM((layers, n, heads, 2 * rows), F32),
             pltpu.VMEM((layers, nc, rows, share), BF16),
             pltpu.VMEM((layers, nc, rows, share), BF16),
@@ -649,18 +750,19 @@
             pltpu.VMEM((be, he), BF16),
             pltpu.VMEM((rows, share), F32),
             pltpu.VMEM((rows, 2 * cols), F32),
+            pltpu.VMEM((nc // 2 + 1, rows, share), F32),
             dma((3 * XPARTS + 6 * layers + 1,)),
-            dma((layers, 4)),
+            dma((layers, 5)),
             dma((layers,)),
             dma((layers, 3)),
             dma((n,)),
             dma((nc + 2,)),
-            dma((n,)),
-            dma((nc,)),
+            dma((2, n)),
+            dma((1,)),
             dma((1,)),
             dma((nc,)),
-            dma((nc // 2,)),
-            dma((nc // 2,)),
+            dma((2, nc // 2)),
+            dma((2, nc // 2)),
         ],
         compiler_params=pltpu.CompilerParams(
             collective_id=0, has_side_effects=True, vmem_limit_bytes=58500000

time: 80.3 us -> 75.4 us (0.939)
  Pallas kernels: 79.5 us -> 74.6 us
    pallas_call x1, Pallas kernels: 76.1 us -> 71.3 us  [local(): pl.pallas_call(functools.partial(kernel, n, head_dim), name='retention',...]
where the time goes in v3:
time: 75.4 us; the launch traced here: 75.3 us
  Pallas kernels  74.6 us (99%)
    pallas_call x1, Pallas kernels, local(): pl.pallas_call(functools.partial(kernel, n, head_dim), name='retention',...  71.3 us
    pallas_call x1, Pallas kernels, local(): pl.pallas_call(store_kernel, name='store', out_shape=(jax.ShapeDtypeStruc...  3.38 us

profile of v3, /device:TPU:0, one launch (start us, length us, event | category | flops | bytes accessed | tf_op | source)
XLA Modules:
  0.0 75.3 jit_solution(8065347458506932692)
XLA Ops:
  0.6 71.3 %retention.1 = (bf16[128,256]{1,0:T(8,128)(2,1)S(1)}, f32[2,32,8,16,256]{4,3,2,1,0:T(8,128)S(1)}) custom-call(bf16[32,4,4096]{2,1,0:T(4,128)(2,1)} %x_hbm.1, f32[2,32,8,16,256]{4,3,2,1,0:T(8,128)} %st_hbm.1, bf16[2,4096]{1,0:T(2,128)(2,1)} %ng_hbm.1, bf16[2,4096,128]{2,1,0:T(8,128)(2,1)} %qw_hbm.1, bf16[2,4096,128]{2,1,0:T(8,128)(2,1)} %kw_hbm.1, ...), custom_call_target="tpu_custom_call" | custom-call | tf_op jit(solution)/shard_map/retention/pallas_call | solution.py:717
  71.9 3.4 %store.1 = (bf16[32,4,256]{2,1,0:T(4,128)(2,1)}, f32[2,32,8,16,256]{4,3,2,1,0:T(8,128)}) custom-call(bf16[128,256]{1,0:T(8,128)(2,1)S(1)} %get-tuple-element.4.y_ref, f32[2,32,8,16,256]{4,3,2,1,0:T(8,128)S(1)} %get-tuple-element.5.state_ref), custom_call_target="tpu_custom_call" | custom-call | tf_op jit(solution)/shard_map/store/pallas_call | solution.py:775

commit v4 on v3

--- a/solution.py
+++ b/solution.py
@@ -148,6 +148,14 @@
     )
 
 
+def thirds(value, axis):
+    high = value.astype(BF16)
+    rest = value - high.astype(F32)
+    middle = rest.astype(BF16)
+    low = (rest - middle.astype(F32)).astype(BF16)
+    return jnp.concatenate([high, middle, low], axis=axis)
+
+
 def log2(value):
     return int(value).bit_length() - 1
 
@@ -174,7 +182,7 @@
     n, head_dim,
     x_hbm, st_hbm, ng_hbm, qw_hbm, kw_hbm, vw_hbm, gw_hbm, gg_hbm, ow_hbm, tab_hbm,
     y_ref, stv,
-    ng_ref, gg_ref, tab_ref, xr, xs, nv, wqk, wvg, wo, qg, kg, sc, vts, vb, sb, pbs, pbr, yss, ysr, rss, rsr, mkc, mks, fold, sqa, qka, osum,
+    ng_ref, gg_ref, tab_ref, xr, xs, nv, wqk, wvg, wo, qg, kg, sc, vts, vb, sb, pbs, pbr, yss, ysr, rss, rsr, mkc, mks, fold, sqa, qka, vga, osum,
     lsem, ag_s, st_s, rs_s, aq_r, ak_r, ax_r, sc_r, st_r, pb_r, ys_r, rs_r,
 ):
     layers, seqs, heads, e_dim, _ = st_hbm.shape
@@ -291,7 +299,7 @@
     drains = []
     halves = [pl.ds(i * (rows // 2), rows // 2) for i in range(2)]
 
-    def ring(name, buf, recv, send, at=None):
+    def ring(name, buf, recv, send, at=None, direct=()):
         def slot_of(j):
             return buf.at[j] if at is None else buf.at[j, at]
 
@@ -318,13 +326,16 @@
             with scope(f"{name}z{o}"):
                 slot = slot_of(at_z(o, yy, core))
                 arrive(slot, o)
-                push(slot, nz + o, facing)
+                if o not in direct:
+                    push(slot, nz + o, facing)
                 push(slot, last(nc + o), partner)
 
         def from_y(o):
             with scope(f"{name}y{o}"):
                 slot = slot_of(at_z(o, 1 - yy, core))
                 arrive(slot, nz + o)
+                for far_o in direct if o == 0 else ():
+                    push(slot, nz + far_o, at_z(far_o, yy, core))
                 push(slot, last(nc + nz + o), partner)
 
         def done(o, side):
@@ -337,7 +348,7 @@
 
         return start, from_z, from_y, done, done_rest
 
-    def in_order(name, from_z, from_y, done, on_chip, between=lambda: None):
+    def in_order(name, from_z, from_y, done, on_chip, early, between, later):
         def use(*which):
             for o, side in which:
                 done(o, side)
@@ -347,6 +358,7 @@
         use((0, 0))
         from_z(near[0])
         from_y(0)
+        early()
         for o in near[1:]:
             from_z(o)
         use((near[0], 0), (0, 1))
@@ -356,6 +368,7 @@
             from_y(o)
         between()
         from_y(near[-1])
+        later()
         use(*[(o, 1) for o in near[:-1]])
         use((near[-1], 1))
 
@@ -380,6 +393,8 @@
             parts.append(scaled)
         both = jnp.concatenate(parts, axis=1) if count > 1 else parts[0]
         qka[...] += jnp.dot(both, wqk[l, at, :], preferred_element_type=F32)
+        if l:
+            vga[...] += nt_dot(both, wvg[l, :, at])
 
     def unpack(j):
         block = xr[:, :, pl.ds(j * share, share)].astype(F32).reshape(rows, share)
@@ -389,6 +404,7 @@
     def clear():
         sqa[...] = jnp.zeros_like(sqa)
         qka[...] = jnp.zeros_like(qka)
+        vga[...] = jnp.zeros_like(vga)
 
     for l in range(layers):
         if l == 0:
@@ -435,15 +451,20 @@
         k_start(other_core=False)
 
         with scope(f"vg{l}"):
-            loads[("v", l)].wait()
-            loads[("g", l)].wait()
-            vg = nt_dot(nv[...], wvg[l]) * scale
-            values = vg[:, :he].astype(BF16)
-            gates = vg[:, he:].astype(BF16).astype(F32)
+            if l == 0:
+                loads[("v", l)].wait()
+                vga[:, :he] = nt_dot(nv[...], wvg[l, :he])
+            values = (vga[:, :he] * scale).astype(BF16)
             vts[...] = jnp.transpose(values.astype(F32)).astype(BF16)
             vb[...] = jnp.dot(nth, values, preferred_element_type=F32).reshape(tok, rows, he)
             loads[("s", l)].wait()
         box = {"mixed": jnp.zeros((rows, he), F32)}
+
+        def gate_on(l=l):
+            if l == 0:
+                with scope(f"gates{l}"):
+                    loads[("g", l)].wait()
+                    vga[:, he:] = nt_dot(nv[...], wvg[l, he:])
 
         def carry_one(o, side, l=l):
             h = chip_at(o, 1 - yy if side else yy)
@@ -463,25 +484,30 @@
                 )
                 box["mixed"] = box["mixed"] + jnp.sum(wide.reshape(tok, rows, he) * vb[...], axis=0)
 
+        def k_on(k_z=k_z, k_y=k_y):
+            for o in near:
+                k_z(o)
+            k_y(0)
+
         def mix(which, box=box):
             for o, side in which:
                 box["mixed"] = box["mixed"] + carry_one(o, side)
 
-        in_order(f"q{l}", q_z, q_y, lambda o, s: None if o == s == 0 else q_done(o, s), mix, intra)
+        in_order(f"q{l}", q_z, q_y, lambda o, s: None if o == s == 0 else q_done(o, s), mix, gate_on, intra, k_on)
         mixed = box["mixed"]
 
         with scope(f"sums{l}"):
-            sums = nt_dot(heads_of, mixed, highest)
-            squares = nt_dot(heads_of, mixed * mixed, highest)
-            sb[l, me] = jnp.concatenate([sums, squares], axis=1)
+            both = nt_dot(
+                jnp.concatenate([heads_of.astype(BF16)] * 3, axis=1),
+                thirds(jnp.concatenate([mixed, mixed * mixed], axis=0), 1),
+            )
+            sums = both[:, :rows]
+            squares = jnp.maximum(both[:, rows:] - sums * sums / e_dim, 0.0)
+            sb[l, me] = jnp.concatenate([sums, squares], axis=1).astype(BF16)
             peers = [at_z(o, y, c) for o in far for y in (1 - yy, yy) for c in (core, 1 - core)]
             for device in peers + [at_z(0, 1 - yy, 1 - core), facing, partner]:
                 remote(sb.at[l, me], sb.at[l, me], st_s.at[l], st_r.at[0], device).start()
             drains.append((sb.at[l, pl.ds(0, n - 1)], st_s.at[l]))
-
-        for o in near:
-            k_z(o)
-        k_y(0)
 
         def update(h, carry, l=l):
             at = pl.ds(pl.multiple_of(h * e_dim, e_dim), e_dim)
@@ -494,6 +520,7 @@
             return carry
 
         with scope(f"silu{l}"):
+            gates = (vga[:, he:] * scale).astype(BF16).astype(F32)
             gain = jnp.dot(gg_ref[l].astype(F32), place, preferred_element_type=F32, precision=highest)
             gain = jnp.sum(gain * heads_of, axis=0, keepdims=True)
             gains = gates / (1.0 + jnp.exp(-gates)) * gain
@@ -503,18 +530,17 @@
             remote(others, others, st_s.at[l], st_r.at[0], partner).wait_recv()
 
         with scope(f"gated{l}"):
-            stats = jnp.sum(sb[l], axis=0)
-            mean = stats[:, :rows] / head_dim
-            var = stats[:, rows:] / head_dim - mean * mean
-            rstd = lax.rsqrt(var + EPS_GROUP)
-
-            def expand(small):
-                return lax.dot_general(
-                    small, heads_of, (((0,), (0,)), ((), ())),
-                    preferred_element_type=F32, precision=highest,
-                )
-
-            gated = ((mixed - expand(mean)) * expand(rstd) * gains).astype(BF16)
+            stats = sb[l].astype(F32)
+            sums = stats[:, :, :rows]
+            total = jnp.sum(sums, axis=0)
+            off = sums - (total / n)[None]
+            var = jnp.sum(stats[:, :, rows:] + off * off / e_dim, axis=0) / head_dim
+            both = jnp.concatenate([total / head_dim, lax.rsqrt(var + EPS_GROUP)], axis=1)
+            both = lax.dot_general(
+                thirds(both, 0), jnp.concatenate([heads_of.astype(BF16)] * 3, axis=0),
+                (((0,), (0,)), ((), ())), preferred_element_type=F32,
+            )
+            gated = ((mixed - both[:rows]) * both[rows:] * gains).astype(BF16)
             loads[("o", l)].wait()
 
         def chunk(j, l=l, gated=gated):
@@ -623,13 +649,15 @@
         rings = []
         clear()
         for i, at in enumerate(halves):
-            rings.append(ring(f"x{l}{i}", xs.at[l + 1], ax_r.at[i], ag_s.at[l, 3 + i], at))
+            rings.append(ring(f"x{l}{i}", xs.at[l + 1], ax_r.at[i], ag_s.at[l, 3 + i], at, (near[-1],) if i else ()))
             if i:
                 join(0, tail)
             xs[l + 1, me, at] = finish(at)
             rings[i][0]()
         loads[("q", l + 1, 0)].wait()
         loads[("k", l + 1, 0)].wait()
+        loads[("v", l + 1)].wait()
+        loads[("g", l + 1)].wait()
         (_, az, ay, ad, _), (_, bz, by, bd, _) = rings
 
         def use(*which, l=l):
@@ -738,7 +766,7 @@
             pltpu.VMEM((layers, heads, 8, rows), F32),
             pltpu.VMEM((he, rows), BF16),
             pltpu.VMEM((tok, rows, he), F32),
-            pltpu.VMEM((layers, n, heads, 2 * rows), F32),
+            pltpu.VMEM((layers, n, heads, 2 * rows), BF16),
             pltpu.VMEM((layers, nc, rows, share), BF16),
             pltpu.VMEM((layers, nc, rows, share), BF16),
             pltpu.VMEM((layers, nc // 2, rows, share), BF16),
@@ -750,6 +778,7 @@
             pltpu.VMEM((be, he), BF16),
             pltpu.VMEM((rows, share), F32),
             pltpu.VMEM((rows, 2 * cols), F32),
+            pltpu.VMEM((rows, 2 * he), F32),
             pltpu.VMEM((nc // 2 + 1, rows, share), F32),
             dma((3 * XPARTS + 6 * layers + 1,)),
             dma((layers, 5)),

time: 75.4 us -> 72.7 us (0.964)
  Pallas kernels: 74.6 us -> 72 us
    pallas_call x1, Pallas kernels: 71.3 us -> 68.6 us  [local(): pl.pallas_call(functools.partial(kernel, n, head_dim), name='retention',...]
where the time goes in v4:
time: 72.7 us; the launch traced here: 72.6 us
  Pallas kernels  72 us (99%)
    pallas_call x1, Pallas kernels, local(): pl.pallas_call(functools.partial(kernel, n, head_dim), name='retention',...  68.6 us
    pallas_call x1, Pallas kernels, local(): pl.pallas_call(store_kernel, name='store', out_shape=(jax.ShapeDtypeStruc...  3.38 us

profile of v4, /device:TPU:0, one launch (start us, length us, event | category | flops | bytes accessed | tf_op | source)
XLA Modules:
  0.0 72.6 jit_solution(8929258411797665898)
XLA Ops:
  0.6 68.6 %retention.1 = (bf16[128,256]{1,0:T(8,128)(2,1)S(1)}, f32[2,32,8,16,256]{4,3,2,1,0:T(8,128)S(1)}) custom-call(bf16[32,4,4096]{2,1,0:T(4,128)(2,1)} %x_hbm.1, f32[2,32,8,16,256]{4,3,2,1,0:T(8,128)} %st_hbm.1, bf16[2,4096]{1,0:T(2,128)(2,1)} %ng_hbm.1, bf16[2,4096,128]{2,1,0:T(8,128)(2,1)} %qw_hbm.1, bf16[2,4096,128]{2,1,0:T(8,128)(2,1)} %kw_hbm.1, ...), custom_call_target="tpu_custom_call" | custom-call | tf_op jit(solution)/shard_map/retention/pallas_call | solution.py:745
  69.2 3.4 %store.1 = (bf16[32,4,256]{2,1,0:T(4,128)(2,1)}, f32[2,32,8,16,256]{4,3,2,1,0:T(8,128)}) custom-call(bf16[128,256]{1,0:T(8,128)(2,1)S(1)} %get-tuple-element.4.y_ref, f32[2,32,8,16,256]{4,3,2,1,0:T(8,128)S(1)} %get-tuple-element.5.state_ref), custom_call_target="tpu_custom_call" | custom-call | tf_op jit(solution)/shard_map/store/pallas_call | solution.py:804

commit v5 on v4

--- a/solution.py
+++ b/solution.py
@@ -234,10 +234,17 @@
         count += 1
 
     wide = width // XPARTS
+
+    def load_queries(l, deep, j):
+        at = pl.ds(j * deep, deep)
+        load(("q", l, j), qw_hbm.at[l, at], wqk.at[l, at, pl.ds(0, cols)])
+        load(("k", l, j), kw_hbm.at[l, at], wqk.at[l, at, pl.ds(cols, cols)])
+
+    load("ng", ng_hbm, ng_ref)
     for j in range(XPARTS):
         at = pl.ds(j * wide, wide)
         load(("x", j), x_hbm.at[:, :, at], xr.at[:, :, at])
-    load("ng", ng_hbm, ng_ref)
+        load_queries(0, wide, j)
 
     barrier = pltpu.get_barrier_semaphore()
     for o in range(1, n):
@@ -246,19 +253,17 @@
             device_id_type=pl.DeviceIdType.MESH,
         )
 
-    for l in range(layers):
-        deep = wide if l == 0 else width
-        for j in range(width // deep):
-            at = pl.ds(j * deep, deep)
-            load(("q", l, j), qw_hbm.at[l, at], wqk.at[l, at, pl.ds(0, cols)])
-            load(("k", l, j), kw_hbm.at[l, at], wqk.at[l, at, pl.ds(cols, cols)])
-        load(("v", l), vw_hbm.at[l], wvg.at[l, pl.ds(0, he)])
-        load(("g", l), gw_hbm.at[l], wvg.at[l, pl.ds(he, he)])
-        load(("s", l), st_hbm.at[l], stv.at[l])
-        load(("o", l), ow_hbm.at[l], wo.at[l])
-        if l == 0:
-            load("tab", tab_hbm, tab_ref)
-            load("gg", gg_hbm, gg_ref)
+    def load_rest():
+        for l in range(layers):
+            if l:
+                load_queries(l, width, 0)
+            load(("v", l), vw_hbm.at[l], wvg.at[l, pl.ds(0, he)])
+            load(("g", l), gw_hbm.at[l], wvg.at[l, pl.ds(he, he)])
+            load(("s", l), st_hbm.at[l], stv.at[l])
+            if l == 0:
+                load("tab", tab_hbm, tab_ref)
+                load("gg", gg_hbm, gg_ref)
+            load(("o", l), ow_hbm.at[l], wo.at[l])
 
     be = seqs * e_dim
 
@@ -299,7 +304,7 @@
     drains = []
     halves = [pl.ds(i * (rows // 2), rows // 2) for i in range(2)]
 
-    def ring(name, buf, recv, send, at=None, direct=()):
+    def ring(name, buf, recv, send, at=None, direct=(), twice=()):
         def slot_of(j):
             return buf.at[j] if at is None else buf.at[j, at]
 
@@ -328,6 +333,8 @@
                 arrive(slot, o)
                 if o not in direct:
                     push(slot, nz + o, facing)
+                if o in twice:
+                    push(slot, nc + nz + o, at_z(0, 1 - yy, 1 - core))
                 push(slot, last(nc + o), partner)
 
         def from_y(o):
@@ -336,7 +343,8 @@
                 arrive(slot, nz + o)
                 for far_o in direct if o == 0 else ():
                     push(slot, nz + far_o, at_z(far_o, yy, core))
-                push(slot, last(nc + nz + o), partner)
+                if o not in twice:
+                    push(slot, last(nc + nz + o), partner)
 
         def done(o, side):
             with scope(f"{name}d{side}{o}"):
@@ -383,23 +391,25 @@
     def absorb(l, j, count, block_of):
         at = pl.ds(pl.multiple_of(j * share, share), share * count)
         parts = []
+        square = sqa[...]
         for i in range(count):
             block = block_of(j + i)
-            sqa[...] += block * block
+            for k in range(0, share, 128):
+                square = square + block[:, k : k + 128] * block[:, k : k + 128]
             one = pl.ds(pl.multiple_of((j + i) * share, share), share)
             gain = ng_ref[l : l + 1, one].astype(F32)
             scaled = (block * gain).astype(BF16)
             nv[:, one] = scaled
             parts.append(scaled)
+        sqa[...] = square
         both = jnp.concatenate(parts, axis=1) if count > 1 else parts[0]
         qka[...] += jnp.dot(both, wqk[l, at, :], preferred_element_type=F32)
         if l:
             vga[...] += nt_dot(both, wvg[l, :, at])
 
     def unpack(j):
-        block = xr[:, :, pl.ds(j * share, share)].astype(F32).reshape(rows, share)
-        xs[0, j] = block.astype(BF16)
-        return block
+        at = pl.ds(j * share if isinstance(j, int) else pl.multiple_of(j * share, share), share)
+        return xr[:, :, at].astype(F32).reshape(rows, share)
 
     def clear():
         sqa[...] = jnp.zeros_like(sqa)
@@ -413,8 +423,11 @@
                 per = n // XPARTS
                 loads["ng"].wait()
                 for p in range(XPARTS):
-                    for name in (("x", p), ("q", 0, p), ("k", 0, p)):
-                        loads[name].wait()
+                    with scope(f"await{p}"):
+                        for name in (("x", p), ("q", 0, p), ("k", 0, p)):
+                            loads[name].wait()
+                    if p == XPARTS - 1:
+                        load_rest()
                     absorb(0, p * per, per, unpack)
 
         with scope(f"qk{l}"):
@@ -426,13 +439,14 @@
             with scope("bar"):
                 pl.semaphore_wait(barrier, n - 1)
 
-        q_start, q_z, q_y, q_done, _ = ring(f"q{l}", qg.at[l], aq_r, ag_s.at[l, 0])
+        q_start, q_z, q_y, q_done, _ = ring(f"q{l}", qg.at[l], aq_r, ag_s.at[l, 0], None, (), (near[-1],))
         k_start, k_z, k_y, k_done, k_rest = ring(f"k{l}", kg.at[l], ak_r, ag_s.at[l, 1])
         q_start()
         k_start(others=False)
         if l == 0:
             with scope("masks"):
                 make_masks()
+                xs[0, me] = unpack(me).astype(BF16)
                 loads["tab"].wait()
                 loads["gg"].wait()
         q_done(0, 0)
@@ -547,7 +561,7 @@
             at = pl.ds(pl.multiple_of(j * share, share), share)
             return jnp.dot(gated, wo[l, :, at], preferred_element_type=F32)
 
-        order = far + [0]
+        order = list(range(nz - 1, -1, -1))
         pb_s, ys_s, rz_s = rs_s.at[l, 0], rs_s.at[l, 1], rs_s.at[l, 2]
 
         def offer(o, side, l=l):
@@ -631,12 +645,12 @@
 
         for o in order:
             join(o, halves[0])
-        for o in later[:-1]:
-            join(o, tail)
         with scope(f"cross{l}"):
             cross().wait_recv()
             yss[l, 0, tail] = (osum[nz, tail] + rsr[l, 0, tail].astype(F32)).astype(BF16)
             hop(0, tail).start()
+        for o in later[:-1]:
+            join(o, tail)
         k_rest()
         with scope(f"update{l}"):
             lax.fori_loop(0, heads, update, 0, unroll=True)
@@ -686,11 +700,11 @@
         use((first, 0), (0, 1))
         by(first)
         use(*[(o, 0) for o in rest])
+        by(end)
         for o in rest[:-1]:
             by(o)
-        by(end)
-        use(*[(o, 1) for o in near[:-1]])
-        use((end, 1))
+        use((first, 1), (end, 1))
+        use(*[(o, 1) for o in rest[:-1]])
 
     with scope("drain"):
         for ref, sem in drains:
@@ -776,7 +790,7 @@
             pltpu.VMEM((rows, be), BF16),
             pltpu.VMEM((be, rows), BF16),
             pltpu.VMEM((be, he), BF16),
-            pltpu.VMEM((rows, share), F32),
+            pltpu.VMEM((rows, 128), F32),
             pltpu.VMEM((rows, 2 * cols), F32),
             pltpu.VMEM((rows, 2 * he), F32),
             pltpu.VMEM((nc // 2 + 1, rows, share), F32),

time: 72.7 us -> 71.2 us (0.979)
  Pallas kernels: 72 us -> 70.3 us
    pallas_call x1, Pallas kernels: 68.6 us -> 66.9 us  [local(): pl.pallas_call(functools.partial(kernel, n, head_dim), name='retention',...]
where the time goes in v5:
time: 71.2 us; the launch traced here: 70.9 us
  Pallas kernels  70.3 us (99%)
    pallas_call x1, Pallas kernels, local(): pl.pallas_call(functools.partial(kernel, n, head_dim), name='retention',...  66.9 us
    pallas_call x1, Pallas kernels, local(): pl.pallas_call(store_kernel, name='store', out_shape=(jax.ShapeDtypeStruc...  3.38 us

profile of v5, /device:TPU:0, one launch (start us, length us, event | category | flops | bytes accessed | tf_op | source)
XLA Modules:
  0.0 70.9 jit_solution(15601536485846125894)
XLA Ops:
  0.6 66.9 %retention.1 = (bf16[128,256]{1,0:T(8,128)(2,1)S(1)}, f32[2,32,8,16,256]{4,3,2,1,0:T(8,128)S(1)}) custom-call(bf16[32,4,4096]{2,1,0:T(4,128)(2,1)} %x_hbm.1, f32[2,32,8,16,256]{4,3,2,1,0:T(8,128)} %st_hbm.1, bf16[2,4096]{1,0:T(2,128)(2,1)} %ng_hbm.1, bf16[2,4096,128]{2,1,0:T(8,128)(2,1)} %qw_hbm.1, bf16[2,4096,128]{2,1,0:T(8,128)(2,1)} %kw_hbm.1, ...), custom_call_target="tpu_custom_call" | custom-call | tf_op jit(solution)/shard_map/retention/pallas_call | solution.py:759
  67.5 3.4 %store.1 = (bf16[32,4,256]{2,1,0:T(4,128)(2,1)}, f32[2,32,8,16,256]{4,3,2,1,0:T(8,128)}) custom-call(bf16[128,256]{1,0:T(8,128)(2,1)S(1)} %get-tuple-element.4.y_ref, f32[2,32,8,16,256]{4,3,2,1,0:T(8,128)S(1)} %get-tuple-element.5.state_ref), custom_call_target="tpu_custom_call" | custom-call | tf_op jit(solution)/shard_map/store/pallas_call | solution.py:818

commit v6 on v5

--- a/solution.py
+++ b/solution.py
@@ -183,7 +183,7 @@
     x_hbm, st_hbm, ng_hbm, qw_hbm, kw_hbm, vw_hbm, gw_hbm, gg_hbm, ow_hbm, tab_hbm,
     y_ref, stv,
     ng_ref, gg_ref, tab_ref, xr, xs, nv, wqk, wvg, wo, qg, kg, sc, vts, vb, sb, pbs, pbr, yss, ysr, rss, rsr, mkc, mks, fold, sqa, qka, vga, osum,
-    lsem, ag_s, st_s, rs_s, aq_r, ak_r, ax_r, sc_r, st_r, pb_r, ys_r, rs_r,
+    lsem, ag_s, st_s, rs_s, aq_r, ak_r, ax_r, am_r, sc_r, st_r, pb_r, ys_r, rs_r,
 ):
     layers, seqs, heads, e_dim, _ = st_hbm.shape
     tok = x_hbm.shape[1]
@@ -216,6 +216,7 @@
 
     facing = at_z(0, 1 - yy, core)
     far = list(range(2, nz)) + [1]
+    xnear = list(range(1, nz))
     near = [1] + list(range(nz - 1, 1, -1))
 
     def remote(src, dst, ssem, rsem, device):
@@ -302,14 +303,18 @@
         ).astype(F32).astype(BF16)
 
     drains = []
+    most = xs.at[0, pl.ds(0, n - 1)]
     halves = [pl.ds(i * (rows // 2), rows // 2) for i in range(2)]
 
-    def ring(name, buf, recv, send, at=None, direct=(), twice=()):
+    def ring(name, buf, recv, send, at=None, direct=(), twice=(), near=near, meet=None):
         def slot_of(j):
             return buf.at[j] if at is None else buf.at[j, at]
 
+        def sem(k):
+            return recv.at[k] if meet is None or k < nc else am_r.at[meet[k - nc]]
+
         def push(slot, k, device):
-            remote(slot, slot, send, recv.at[k], device).start()
+            remote(slot, slot, send, sem(k), device).start()
 
         def arrive(slot, k):
             remote(slot, slot, send, recv.at[k], partner).wait_recv()
@@ -322,10 +327,9 @@
                 push(own, nz, facing)
                 for o in near:
                     push(own, o, at_z(o, yy, core))
-                drains.append((slot_of(pl.ds(0, n - 1)), send))
 
         def last(k):
-            return k if recv.shape[0] == n else nc if k == nc else nc + 1
+            return nc + 1 if recv.shape[0] == nc + 2 and k > nc else k
 
         def from_z(o):
             with scope(f"{name}z{o}"):
@@ -439,8 +443,9 @@
             with scope("bar"):
                 pl.semaphore_wait(barrier, n - 1)
 
-        q_start, q_z, q_y, q_done, _ = ring(f"q{l}", qg.at[l], aq_r, ag_s.at[l, 0], None, (), (near[-1],))
-        k_start, k_z, k_y, k_done, k_rest = ring(f"k{l}", kg.at[l], ak_r, ag_s.at[l, 1])
+        q_start, q_z, q_y, q_done, _ = ring(f"q{l}", qg.at[l], aq_r, ag_s.at[l], None, (), (near[-1],))
+        k_start, k_z, k_y, k_done, k_rest = ring(f"k{l}", kg.at[l], ak_r, ag_s.at[l])
+        drains.append((most, ag_s.at[l]))
         q_start()
         k_start(others=False)
         if l == 0:
@@ -458,10 +463,10 @@
             for o, side in [(o, side) for o in far for side in (1, 0)] + [(0, 1)]:
                 slot = sc.at[l, chip]
                 remote(
-                    slot, slot, ag_s.at[l, 2], sc_r.at[0],
+                    slot, slot, ag_s.at[layers + l], sc_r.at[0],
                     at_z(o, 1 - yy if side else yy, core),
                 ).start()
-            drains.append((sc.at[l, pl.ds(0, nc - 1)], ag_s.at[l, 2]))
+            drains.append((sc.at[l, pl.ds(0, nc - 1)], ag_s.at[layers + l]))
         k_start(other_core=False)
 
         with scope(f"vg{l}"):
@@ -491,7 +496,7 @@
         def intra(l=l, box=box):
             with scope(f"intra{l}"):
                 others = sc.at[l, pl.ds(0, nc - 1)]
-                remote(others, others, ag_s.at[l, 2], sc_r.at[0], partner).wait_recv()
+                remote(others, others, ag_s.at[layers + l], sc_r.at[0], partner).wait_recv()
                 flat = jnp.concatenate([sc[l, :, t, :] for t in range(tok)], axis=1).astype(BF16)
                 wide = lax.dot_general(
                     flat, heads_of.astype(BF16), (((0,), (0,)), ((), ())), preferred_element_type=F32
@@ -562,7 +567,7 @@
             return jnp.dot(gated, wo[l, :, at], preferred_element_type=F32)
 
         order = list(range(nz - 1, -1, -1))
-        pb_s, ys_s, rz_s = rs_s.at[l, 0], rs_s.at[l, 1], rs_s.at[l, 2]
+        pb_s = ys_s = rz_s = rs_s.at[l]
 
         def offer(o, side, l=l):
             k = side * nz + o
@@ -586,10 +591,10 @@
 
         def turn(o, at, l=l):
             src, dst = rss.at[l, o, at], rsr.at[l, o, at]
-            return remote(src, dst, rz_s, rs_r.at[halves.index(at), o], at_z(o, yy, core))
+            return remote(src, dst, rz_s, rs_r.at[halves.index(at)], at_z(o, yy, core))
 
         def cross(l=l):
-            return remote(rss.at[l, 0, tail], rsr.at[l, 0, tail], rz_s, rs_r.at[1, 0], at_z(early, yy, core))
+            return remote(rss.at[l, 0, tail], rsr.at[l, 0, tail], rz_s, rs_r.at[2], at_z(early, yy, core))
 
         with scope(f"rsa{l}"):
             offer(early, 1)
@@ -618,9 +623,7 @@
                 offer(o, 0)
             for o in near:
                 k_y(o)
-            drains.append((pbs.at[l], pb_s))
-            drains.append((pbs.at[l, pl.ds(0, 2 * nz - 1), tail], ys_s))
-            drains.append((pbs.at[l, pl.ds(0, 2 * nz - 1), tail], rz_s))
+            drains.append((most, rs_s.at[l]))
         with scope(f"own{l}"):
             for o in later:
                 osum[o] = paired(o, 0)
@@ -638,8 +641,9 @@
         def finish(at, l=l):
             acc = osum[0, at] + xs[l, me, at].astype(F32)
             with scope(f"rse{l}"):
+                parts = rsr.at[l, pl.ds(1, nz - 1), at]
+                remote(parts, parts, rz_s, rs_r.at[halves.index(at)], facing).wait_recv()
                 for o in near:
-                    turn(o, at).wait_recv()
                     acc = acc + rsr[l, o, at].astype(F32)
             return acc.astype(BF16)
 
@@ -660,10 +664,15 @@
             y_ref[tail, :] = finish(tail)
             continue
 
+        first, rest, end = xnear[0], xnear[1:], xnear[-1]
+        meet = {0: 0, first: 1, nz: 1, nz + first: 3, nz + end: 3}
+        meet.update({o: 2 for o in rest})
+        meet.update({nz + o: 4 for o in rest[:-1]})
         rings = []
         clear()
+        drains.append((most, ag_s.at[2 * layers + l]))
         for i, at in enumerate(halves):
-            rings.append(ring(f"x{l}{i}", xs.at[l + 1], ax_r.at[i], ag_s.at[l, 3 + i], at, (near[-1],) if i else ()))
+            rings.append(ring(f"x{l}{i}", xs.at[l + 1], ax_r.at[i], ag_s.at[2 * layers + l], at, (xnear[-1],) if i else (), tuple(xnear[1:-1]) if i else (), xnear, meet))
             if i:
                 join(0, tail)
             xs[l + 1, me, at] = finish(at)
@@ -672,18 +681,18 @@
         loads[("k", l + 1, 0)].wait()
         loads[("v", l + 1)].wait()
         loads[("g", l + 1)].wait()
-        (_, az, ay, ad, _), (_, bz, by, bd, _) = rings
+        (_, az, ay, _, _), (_, bz, by, _, _) = rings
 
         def use(*which, l=l):
-            for o, side in which:
-                ad(o, side)
-                bd(o, side)
+            o, side = which[0]
+            both = xs.at[l + 1, pl.ds(0, len(which))]
+            with scope(f"x{l}d{side}{o}"):
+                remote(both, both, ag_s.at[2 * layers + l], am_r.at[meet[side * nz + o]], partner).wait_recv()
             with scope(f"x{l}c{which[0][1]}{which[0][0]}"):
                 for o, side in which:
                     c = chip_at(o, 1 - yy if side else yy)
                     absorb(l + 1, 2 * c, 2, lambda j: xs[l + 1, j].astype(F32))
 
-        first, rest, end = near[0], near[1:], near[-1]
         az(first)
         ay(0)
         for o in rest:
@@ -701,9 +710,9 @@
         by(first)
         use(*[(o, 0) for o in rest])
         by(end)
+        use((first, 1), (end, 1))
         for o in rest[:-1]:
             by(o)
-        use((first, 1), (end, 1))
         use(*[(o, 1) for o in rest[:-1]])
 
     with scope("drain"):
@@ -742,7 +751,7 @@
     fits = (
         cols == 128 and head_dim == 256 and he == 128 and heads == 8 and e_dim == 16
         and share % 128 == 0 and n % 4 == 0 and n & (n - 1) == 0 and rows == 128 and 8 % tok == 0
-        and n == 2 * heads and seqs % 4 == 0
+        and n == 2 * heads and seqs % 4 == 0 and share == 2 * cols
     )
     if not fits:
         return plain_local(
@@ -795,17 +804,18 @@
             pltpu.VMEM((rows, 2 * he), F32),
             pltpu.VMEM((nc // 2 + 1, rows, share), F32),
             dma((3 * XPARTS + 6 * layers + 1,)),
-            dma((layers, 5)),
+            dma((3 * layers - 1,)),
             dma((layers,)),
-            dma((layers, 3)),
+            dma((layers,)),
             dma((n,)),
             dma((nc + 2,)),
-            dma((2, n)),
+            dma((2, nc)),
+            dma((5,)),
             dma((1,)),
             dma((1,)),
             dma((nc,)),
             dma((2, nc // 2)),
-            dma((2, nc // 2)),
+            dma((3,)),
         ],
         compiler_params=pltpu.CompilerParams(
             collective_id=0, has_side_effects=True, vmem_limit_bytes=58500000

time: 71.2 us -> 71.6 us (level)
  no operation moved by 1% of the time
where the time goes in v6:
time: 71.6 us; the launch traced here: 71.3 us
  Pallas kernels  70.7 us (99%)
    pallas_call x1, Pallas kernels, local(): pl.pallas_call(functools.partial(kernel, n, head_dim), name='retention',...  67.3 us
    pallas_call x1, Pallas kernels, local(): pl.pallas_call(store_kernel, name='store', out_shape=(jax.ShapeDtypeStruc...  3.38 us

profile of v6, /device:TPU:0, one launch (start us, length us, event | category | flops | bytes accessed | tf_op | source)
XLA Modules:
  0.0 71.3 jit_solution(11862755054816366040)
XLA Ops:
  0.6 67.3 %retention.1 = (bf16[128,256]{1,0:T(8,128)(2,1)S(1)}, f32[2,32,8,16,256]{4,3,2,1,0:T(8,128)S(1)}) custom-call(bf16[32,4,4096]{2,1,0:T(4,128)(2,1)} %x_hbm.1, f32[2,32,8,16,256]{4,3,2,1,0:T(8,128)} %st_hbm.1, bf16[2,4096]{1,0:T(2,128)(2,1)} %ng_hbm.1, bf16[2,4096,128]{2,1,0:T(8,128)(2,1)} %qw_hbm.1, bf16[2,4096,128]{2,1,0:T(8,128)(2,1)} %kw_hbm.1, ...), custom_call_target="tpu_custom_call" | custom-call | tf_op jit(solution)/shard_map/retention/pallas_call | solution.py:768
  67.9 3.4 %store.1 = (bf16[32,4,256]{2,1,0:T(4,128)(2,1)}, f32[2,32,8,16,256]{4,3,2,1,0:T(8,128)}) custom-call(bf16[128,256]{1,0:T(8,128)(2,1)S(1)} %get-tuple-element.4.y_ref, f32[2,32,8,16,256]{4,3,2,1,0:T(8,128)S(1)} %get-tuple-element.5.state_ref), custom_call_target="tpu_custom_call" | custom-call | tf_op jit(solution)/shard_map/store/pallas_call | solution.py:828

commit v7 on v6

--- a/solution.py
+++ b/solution.py
@@ -182,8 +182,8 @@
     n, head_dim,
     x_hbm, st_hbm, ng_hbm, qw_hbm, kw_hbm, vw_hbm, gw_hbm, gg_hbm, ow_hbm, tab_hbm,
     y_ref, stv,
-    ng_ref, gg_ref, tab_ref, xr, xs, nv, wqk, wvg, wo, qg, kg, sc, vts, vb, sb, pbs, pbr, yss, ysr, rss, rsr, mkc, mks, fold, sqa, qka, vga, osum,
-    lsem, ag_s, st_s, rs_s, aq_r, ak_r, ax_r, am_r, sc_r, st_r, pb_r, ys_r, rs_r,
+    ng_ref, gg_ref, tab_ref, xr, xs, nv, wqk, wvg, wo, qg, kg, sc, vts, vb, sb, wop, mgs, mgr, yss, ysr, rss, rsr, mkc, mks, fold, sqa, qka, vga, osum,
+    lsem, ag_s, st_s, rs_s, aq_r, ak_r, ax_r, am_r, sc_r, st_r, wo_s, mg_s, wo_r, mg_r, ys_r, rs_r,
 ):
     layers, seqs, heads, e_dim, _ = st_hbm.shape
     tok = x_hbm.shape[1]
@@ -468,6 +468,10 @@
                 ).start()
             drains.append((sc.at[l, pl.ds(0, nc - 1)], ag_s.at[layers + l]))
         k_start(other_core=False)
+        for c in range(nc):
+            at = pl.ds(pl.multiple_of((2 * c + 1 - core) * share, share), share)
+            remote(ow_hbm.at[l, :, at], wop.at[l, c], wo_s.at[l], wo_r.at[0], partner).start()
+        drains.append((wop.at[l], wo_s.at[l]))
 
         with scope(f"vg{l}"):
             if l == 0:
@@ -543,6 +547,14 @@
             gain = jnp.dot(gg_ref[l].astype(F32), place, preferred_element_type=F32, precision=highest)
             gain = jnp.sum(gain * heads_of, axis=0, keepdims=True)
             gains = gates / (1.0 + jnp.exp(-gates)) * gain
+            mgs[l, 0] = mixed
+            mgs[l, 1] = gains
+            pair = remote(mgs.at[l], mgr.at[l], mg_s.at[l], mg_r.at[0], partner)
+            pair.start()
+            drains.append((mgs.at[l], mg_s.at[l]))
+            loads[("o", l)].wait()
+            remote(wop.at[l], wop.at[l], wo_s.at[l], wo_r.at[0], partner).wait_recv()
+            pair.wait_recv()
 
         with scope(f"stwait{l}"):
             others = sb.at[l, pl.ds(0, n - 1)]
@@ -560,26 +572,16 @@
                 (((0,), (0,)), ((), ())), preferred_element_type=F32,
             )
             gated = ((mixed - both[:rows]) * both[rows:] * gains).astype(BF16)
-            loads[("o", l)].wait()
-
-        def chunk(j, l=l, gated=gated):
-            at = pl.ds(pl.multiple_of(j * share, share), share)
-            return jnp.dot(gated, wo[l, :, at], preferred_element_type=F32)
+            other = ((mgr[l, 0] - both[:rows]) * both[rows:] * mgr[l, 1]).astype(BF16)
+
+        def paired(o, side, l=l, gated=gated, other=other):
+            c = chip_at(o, 1 - yy if side else yy)
+            at = pl.ds(pl.multiple_of((2 * c + core) * share, share), share)
+            own = jnp.dot(gated, wo[l, :, at], preferred_element_type=F32)
+            return own + jnp.dot(other, wop[l, c], preferred_element_type=F32)
 
         order = list(range(nz - 1, -1, -1))
-        pb_s = ys_s = rz_s = rs_s.at[l]
-
-        def offer(o, side, l=l):
-            k = side * nz + o
-            y = 1 - yy if side else yy
-            pbs[l, k] = chunk(at_z(o, y, 1 - core)).astype(BF16)
-            remote(pbs.at[l, k], pbr.at[l, k], pb_s, pb_r.at[k], partner).start()
-
-        def paired(o, side, l=l):
-            k = side * nz + o
-            own = chunk(at_z(o, 1 - yy if side else yy, core))
-            remote(pbs.at[l, k], pbr.at[l, k], pb_s, pb_r.at[k], partner).wait_recv()
-            return own + pbr[l, k].astype(F32)
+        ys_s = rz_s = rs_s.at[l]
 
         early = order[0]
         later = order[1:]
@@ -596,11 +598,6 @@
         def cross(l=l):
             return remote(rss.at[l, 0, tail], rsr.at[l, 0, tail], rz_s, rs_r.at[2], at_z(early, yy, core))
 
-        with scope(f"rsa{l}"):
-            offer(early, 1)
-            offer(early, 0)
-            for o in later:
-                offer(o, 1)
         with scope(f"rsb{l}"):
             both = paired(early, 1).astype(BF16)
             yss[l, early] = both
@@ -619,11 +616,9 @@
             for o in later[:-1]:
                 hop(o, tail).start()
         with scope(f"rsc{l}"):
-            for o in later:
-                offer(o, 0)
             for o in near:
                 k_y(o)
-            drains.append((most, rs_s.at[l]))
+            drains.append((xs.at[0, pl.ds(0, 2 * nz - 1)], rs_s.at[l]))
         with scope(f"own{l}"):
             for o in later:
                 osum[o] = paired(o, 0)
@@ -790,8 +785,9 @@
             pltpu.VMEM((he, rows), BF16),
             pltpu.VMEM((tok, rows, he), F32),
             pltpu.VMEM((layers, n, heads, 2 * rows), BF16),
-            pltpu.VMEM((layers, nc, rows, share), BF16),
-            pltpu.VMEM((layers, nc, rows, share), BF16),
+            pltpu.VMEM((layers, nc, he, share), BF16),
+            pltpu.VMEM((layers, 2, rows, he), F32),
+            pltpu.VMEM((layers, 2, rows, he), F32),
             pltpu.VMEM((layers, nc // 2, rows, share), BF16),
             pltpu.VMEM((layers, nc // 2, rows, share), BF16),
             pltpu.VMEM((layers, nc // 2, rows, share), BF16),
@@ -813,7 +809,10 @@
             dma((5,)),
             dma((1,)),
             dma((1,)),
-            dma((nc,)),
+            dma((layers,)),
+            dma((layers,)),
+            dma((1,)),
+            dma((1,)),
             dma((2, nc // 2)),
             dma((3,)),
         ],

time: 71.6 us -> 68.9 us (0.962)
  Pallas kernels: 70.7 us -> 68 us
    pallas_call x1, Pallas kernels: 67.3 us -> 64.7 us  [local(): pl.pallas_call(functools.partial(kernel, n, head_dim), name='retention',...]
where the time goes in v7:
time: 68.9 us; the launch traced here: 68.7 us
  Pallas kernels  68 us (99%)
    pallas_call x1, Pallas kernels, local(): pl.pallas_call(functools.partial(kernel, n, head_dim), name='retention',...  64.7 us
    pallas_call x1, Pallas kernels, local(): pl.pallas_call(store_kernel, name='store', out_shape=(jax.ShapeDtypeStruc...  3.38 us

profile of v7, /device:TPU:0, one launch (start us, length us, event | category | flops | bytes accessed | tf_op | source)
XLA Modules:
  0.0 68.7 jit_solution(13307448773885017081)
XLA Ops:
  0.6 64.7 %retention.1 = (bf16[128,256]{1,0:T(8,128)(2,1)S(1)}, f32[2,32,8,16,256]{4,3,2,1,0:T(8,128)S(1)}) custom-call(bf16[32,4,4096]{2,1,0:T(4,128)(2,1)} %x_hbm.1, f32[2,32,8,16,256]{4,3,2,1,0:T(8,128)} %st_hbm.1, bf16[2,4096]{1,0:T(2,128)(2,1)} %ng_hbm.1, bf16[2,4096,128]{2,1,0:T(8,128)(2,1)} %qw_hbm.1, bf16[2,4096,128]{2,1,0:T(8,128)(2,1)} %kw_hbm.1, ...), custom_call_target="tpu_custom_call" | custom-call | tf_op jit(solution)/shard_map/retention/pallas_call | solution.py:763
  65.3 3.4 %store.1 = (bf16[32,4,256]{2,1,0:T(4,128)(2,1)}, f32[2,32,8,16,256]{4,3,2,1,0:T(8,128)}) custom-call(bf16[128,256]{1,0:T(8,128)(2,1)S(1)} %get-tuple-element.4.y_ref, f32[2,32,8,16,256]{4,3,2,1,0:T(8,128)S(1)} %get-tuple-element.5.state_ref), custom_call_target="tpu_custom_call" | custom-call | tf_op jit(solution)/shard_map/store/pallas_call | solution.py:827

commit v8 on v7

--- a/solution.py
+++ b/solution.py
@@ -371,17 +371,18 @@
         from_z(near[0])
         from_y(0)
         early()
-        for o in near[1:]:
+        for o in near[1:-1]:
             from_z(o)
         use((near[0], 0), (0, 1))
+        from_z(near[-1])
         from_y(near[0])
         use(*[(o, 0) for o in near[1:]])
         for o in near[1:-1]:
             from_y(o)
         between()
+        use(*[(o, 1) for o in near[:-1]])
+        later()
         from_y(near[-1])
-        later()
-        use(*[(o, 1) for o in near[:-1]])
         use((near[-1], 1))
 
     def spread(table):
@@ -508,7 +509,7 @@
                 box["mixed"] = box["mixed"] + jnp.sum(wide.reshape(tok, rows, he) * vb[...], axis=0)
 
         def k_on(k_z=k_z, k_y=k_y):
-            for o in near:
+            for o in near[:-1]:
                 k_z(o)
             k_y(0)
 
@@ -542,6 +543,7 @@
             stv[l, :, h] = ((state + fresh) * fade).reshape(seqs, e_dim, head_dim)
             return carry
 
+        k_z(near[-1])
         with scope(f"silu{l}"):
             gates = (vga[:, he:] * scale).astype(BF16).astype(F32)
             gain = jnp.dot(gg_ref[l].astype(F32), place, preferred_element_type=F32, precision=highest)
@@ -642,6 +644,9 @@
                     acc = acc + rsr[l, o, at].astype(F32)
             return acc.astype(BF16)
 
+        k_rest()
+        with scope(f"update{l}"):
+            lax.fori_loop(0, heads, update, 0, unroll=True)
         for o in order:
             join(o, halves[0])
         with scope(f"cross{l}"):
@@ -650,9 +655,6 @@
             hop(0, tail).start()
         for o in later[:-1]:
             join(o, tail)
-        k_rest()
-        with scope(f"update{l}"):
-            lax.fori_loop(0, heads, update, 0, unroll=True)
         if l + 1 == layers:
             y_ref[halves[0], :] = finish(halves[0])
             join(0, tail)

time: 68.9 us -> 68.1 us (0.988)
  Pallas kernels: 68 us -> 67.2 us
    pallas_call x1, Pallas kernels: 64.7 us -> 63.8 us  [local(): pl.pallas_call(functools.partial(kernel, n, head_dim), name='retention',...]
where the time goes in v8:
time: 68.1 us; the launch traced here: 67.9 us
  Pallas kernels  67.2 us (99%)
    pallas_call x1, Pallas kernels, local(): pl.pallas_call(functools.partial(kernel, n, head_dim), name='retention',...  63.8 us
    pallas_call x1, Pallas kernels, local(): pl.pallas_call(store_kernel, name='store', out_shape=(jax.ShapeDtypeStruc...  3.38 us

profile of v8, /device:TPU:0, one launch (start us, length us, event | category | flops | bytes accessed | tf_op | source)
XLA Modules:
  0.0 67.9 jit_solution(6730151370990509186)
XLA Ops:
  0.6 63.8 %retention.1 = (bf16[128,256]{1,0:T(8,128)(2,1)S(1)}, f32[2,32,8,16,256]{4,3,2,1,0:T(8,128)S(1)}) custom-call(bf16[32,4,4096]{2,1,0:T(4,128)(2,1)} %x_hbm.1, f32[2,32,8,16,256]{4,3,2,1,0:T(8,128)} %st_hbm.1, bf16[2,4096]{1,0:T(2,128)(2,1)} %ng_hbm.1, bf16[2,4096,128]{2,1,0:T(8,128)(2,1)} %qw_hbm.1, bf16[2,4096,128]{2,1,0:T(8,128)(2,1)} %kw_hbm.1, ...), custom_call_target="tpu_custom_call" | custom-call | tf_op jit(solution)/shard_map/retention/pallas_call | solution.py:765
  64.5 3.4 %store.1 = (bf16[32,4,256]{2,1,0:T(4,128)(2,1)}, f32[2,32,8,16,256]{4,3,2,1,0:T(8,128)}) custom-call(bf16[128,256]{1,0:T(8,128)(2,1)S(1)} %get-tuple-element.4.y_ref, f32[2,32,8,16,256]{4,3,2,1,0:T(8,128)S(1)} %get-tuple-element.5.state_ref), custom_call_target="tpu_custom_call" | custom-call | tf_op jit(solution)/shard_map/store/pallas_call | solution.py:829

commit v9 on v8

--- a/solution.py
+++ b/solution.py
@@ -421,6 +421,11 @@
         qka[...] = jnp.zeros_like(qka)
         vga[...] = jnp.zeros_like(vga)
 
+    def send_rows(l):
+        for c in range(nc):
+            at = pl.ds(pl.multiple_of((2 * c + 1 - core) * share, share), share)
+            remote(ow_hbm.at[l, :, at], wop.at[l, c], wo_s.at[l], wo_r.at[l], partner).start()
+
     for l in range(layers):
         if l == 0:
             with scope("absorb"):
@@ -469,9 +474,8 @@
                 ).start()
             drains.append((sc.at[l, pl.ds(0, nc - 1)], ag_s.at[layers + l]))
         k_start(other_core=False)
-        for c in range(nc):
-            at = pl.ds(pl.multiple_of((2 * c + 1 - core) * share, share), share)
-            remote(ow_hbm.at[l, :, at], wop.at[l, c], wo_s.at[l], wo_r.at[0], partner).start()
+        if l == 0:
+            send_rows(0)
         drains.append((wop.at[l], wo_s.at[l]))
 
         with scope(f"vg{l}"):
@@ -555,7 +559,7 @@
             pair.start()
             drains.append((mgs.at[l], mg_s.at[l]))
             loads[("o", l)].wait()
-            remote(wop.at[l], wop.at[l], wo_s.at[l], wo_r.at[0], partner).wait_recv()
+            remote(wop.at[l], wop.at[l], wo_s.at[l], wo_r.at[l], partner).wait_recv()
             pair.wait_recv()
 
         with scope(f"stwait{l}"):
@@ -621,6 +625,8 @@
             for o in near:
                 k_y(o)
             drains.append((xs.at[0, pl.ds(0, 2 * nz - 1)], rs_s.at[l]))
+        if l + 1 < layers:
+            send_rows(l + 1)
         with scope(f"own{l}"):
             for o in later:
                 osum[o] = paired(o, 0)
@@ -813,7 +819,7 @@
             dma((1,)),
             dma((layers,)),
             dma((layers,)),
-            dma((1,)),
+            dma((layers,)),
             dma((1,)),
             dma((2, nc // 2)),
             dma((3,)),

time: 68.1 us -> 68.1 us (level)
  no operation moved by 1% of the time
where the time goes in v9:
time: 68.1 us; the launch traced here: 67.9 us
  Pallas kernels  67.2 us (99%)
    pallas_call x1, Pallas kernels, local(): pl.pallas_call(functools.partial(kernel, n, head_dim), name='retention',...  63.9 us
    pallas_call x1, Pallas kernels, local(): pl.pallas_call(store_kernel, name='store', out_shape=(jax.ShapeDtypeStruc...  3.38 us

profile of v9, /device:TPU:0, one launch (start us, length us, event | category | flops | bytes accessed | tf_op | source)
XLA Modules:
  0.0 67.9 jit_solution(8931297009564382470)
XLA Ops:
  0.6 63.9 %retention.1 = (bf16[128,256]{1,0:T(8,128)(2,1)S(1)}, f32[2,32,8,16,256]{4,3,2,1,0:T(8,128)S(1)}) custom-call(bf16[32,4,4096]{2,1,0:T(4,128)(2,1)} %x_hbm.1, f32[2,32,8,16,256]{4,3,2,1,0:T(8,128)} %st_hbm.1, bf16[2,4096]{1,0:T(2,128)(2,1)} %ng_hbm.1, bf16[2,4096,128]{2,1,0:T(8,128)(2,1)} %qw_hbm.1, bf16[2,4096,128]{2,1,0:T(8,128)(2,1)} %kw_hbm.1, ...), custom_call_target="tpu_custom_call" | custom-call | tf_op jit(solution)/shard_map/retention/pallas_call | solution.py:771
  64.5 3.4 %store.1 = (bf16[32,4,256]{2,1,0:T(4,128)(2,1)}, f32[2,32,8,16,256]{4,3,2,1,0:T(8,128)}) custom-call(bf16[128,256]{1,0:T(8,128)(2,1)S(1)} %get-tuple-element.4.y_ref, f32[2,32,8,16,256]{4,3,2,1,0:T(8,128)S(1)} %get-tuple-element.5.state_ref), custom_call_target="tpu_custom_call" | custom-call | tf_op jit(solution)/shard_map/store/pallas_call | solution.py:835
